TPU v7x, 32 devices: a whole 2x2x4 slice. The times are simulated.
32 devices in a mesh: kv: 8 (over z, y), tp: 4 (over x, core).
Axes of the slice: x: 2, y: 2, z: 4, core: 2. Of those that a mesh axis runs over, the one named last changes fastest.
Arguments:
- tokens: bfloat16 [16, 16, 4096], replicated, may hold values from -6 to 6
- gain_pre: float32 [4096], replicated, may hold values from 0.1 to 1.9
- w_query: bfloat16 [4096, 2048], P('kv', 'tp'), may hold values from -0.09375 to 0.09375
- w_key: bfloat16 [4096, 2048], P('kv', 'tp'), may hold values from -0.09375 to 0.09375
- w_value: bfloat16 [4096, 2048], P('kv', 'tp'), may hold values from -0.09375 to 0.09375
- w_forget: bfloat16 [4096, 16], replicated, may hold values from -0.09375 to 0.09375
- b_forget: float32 [16], replicated
- w_out: bfloat16 [2048, 4096], P('tp', 'kv'), may hold values from -0.125 to 0.125
- gain_post: float32 [4096], P(('kv', 'tp')), may hold values from 0.1 to 1.9
- key_cache: bfloat16 [16, 1024, 16, 128], P(None, 'kv', 'tp'), may hold values from -6 to 6
- value_cache: bfloat16 [16, 1024, 16, 128], P(None, 'kv', 'tp'), may hold values from -6 to 6
- cum_cache: float32 [16, 1024, 16], P(None, 'kv', 'tp'), may hold values from -402 to 0, as said below
- lengths: int32 [16], replicated, may hold values from 512 to 992
- accepted: int32 [16], replicated, may hold values from 0 to 16
- parent: int32 [16, 16], replicated, may hold values from -1 to 14, as said below
Outputs:
- mixed: bfloat16 [16, 16, 4096], P(None, None, ('kv', 'tp'))
- key_out: bfloat16 [16, 1024, 16, 128], P(None, 'kv', 'tp')
- value_out: bfloat16 [16, 1024, 16, 128], P(None, 'kv', 'tp')
- cum_out: float32 [16, 1024, 16], P(None, 'kv', 'tp')
Inputs may be any that keep to these rules, and one draw needn't show every extreme that they name: parent[s, 0] is -1 and parent[s, i] lies between -1 and i - 1. `cum_cache`: along the positions of each sequence and head the values never rise. lengths + accepted + 16 never exceeds 1024.
All inputs are finite; a program needn't handle non-finite values.
Results may differ from a plain program's by a relative error of at most 0.03.
Values may be sent and summed in bfloat16 or wider, within the bound.
A program may use at most 64 MiB of HBM per device.

v0:
```python
import functools

import jax
import jax.numpy as jnp
from jax import lax
from jax.experimental import pallas as pl
from jax.experimental.pallas import tpu as pltpu
from jax.sharding import PartitionSpec as P

epsilon = 1e-06
floor_value = -1e30


def merged(part, axis, combine):
    gathered = jax.tree.map(lambda a: lax.all_gather(a, axis), part)

    def take(source):
        return jax.tree.map(lambda a: lax.dynamic_index_in_dim(a, source, 0, False), gathered)

    return lax.fori_loop(
        1, lax.axis_size(axis), lambda source, state: combine(state, take(source)), take(0)
    )


def ancestry(parent_ids, members):
    identity = jnp.eye(members, dtype=jnp.float32)
    parent_hot = (
        parent_ids[:, :, None] == jnp.arange(members, dtype=jnp.int32)[None, None, :]
    ).astype(jnp.float32)
    ancestors = jnp.minimum(identity[None] + parent_hot, 1.0)
    for sweep in range(max(1, (members - 1).bit_length())):
        ancestors = jnp.minimum(
            jnp.einsum("bij,bjk->bik", ancestors, ancestors, precision=lax.Precision.HIGHEST), 1.0
        )
    return ancestors


def combine_parts(first, second):
    new_max = jnp.maximum(first[0], second[0])
    first_scale = jnp.exp(first[0] - new_max)
    second_scale = jnp.exp(second[0] - new_max)
    return (
        new_max,
        first[1] * first_scale + second[1] * second_scale,
        first[2] * first_scale[..., None] + second[2] * second_scale[..., None],
        jnp.maximum(first[3], second[3]),
    )


def finish_rows(cache_max, cache_total, cache_values, last_rows, tree_max, tree_total, tree_values):
    shifted = cache_max + last_rows
    top = jnp.maximum(shifted, tree_max)
    cache_scale = jnp.exp(shifted - top)
    tree_scale = jnp.exp(tree_max - top)
    attended = (
        (cache_values * cache_scale[..., None] + tree_values * tree_scale[..., None])
        / (cache_total * cache_scale + tree_total * tree_scale)[..., None]
    ).astype(jnp.bfloat16)
    return attended.reshape(attended.shape[0], attended.shape[1] * attended.shape[2])


def per_device(
    tokens,
    gain_pre,
    w_query,
    w_key,
    w_value,
    w_forget,
    b_forget,
    w_out,
    gain_post,
    key_cache,
    value_cache,
    cum_cache,
    lengths,
    accepted,
    parent,
):
    num_seqs, proposals, model_width = tokens.shape
    kv_rank = lax.axis_index("kv")
    tp_rank = lax.axis_index("tp")
    span = key_cache.shape[1]
    heads_local = key_cache.shape[2]
    head_dim = key_cache.shape[3]
    scale = head_dim ** (-0.5)
    all_rows = num_seqs * proposals
    tok_float = tokens.astype(jnp.float32)
    normed = (
        tok_float
        * lax.rsqrt(jnp.mean(tok_float * tok_float, -1, keepdims=True) + epsilon)
        * gain_pre
    ).astype(jnp.bfloat16)
    flat = normed.reshape(all_rows, model_width)
    weight_rows = w_query.shape[0]
    local_rows = lax.dynamic_slice_in_dim(flat, kv_rank * weight_rows, weight_rows, 1)
    query_part = jnp.dot(local_rows, w_query, preferred_element_type=jnp.float32)
    key_part = jnp.dot(local_rows, w_key, preferred_element_type=jnp.float32)
    value_part = jnp.dot(local_rows, w_value, preferred_element_type=jnp.float32)
    summed = (
        lax.psum(query_part.astype(jnp.bfloat16), "kv").astype(jnp.float32),
        lax.psum(key_part.astype(jnp.bfloat16), "kv").astype(jnp.float32),
        lax.psum(value_part.astype(jnp.bfloat16), "kv").astype(jnp.float32),
    )
    query_flat = summed[0].astype(jnp.bfloat16)
    key_flat = summed[1].astype(jnp.bfloat16)
    value_flat = summed[2].astype(jnp.bfloat16)
    query = query_flat.reshape(num_seqs, proposals, heads_local, head_dim)
    key_new = key_flat.reshape(num_seqs, proposals, heads_local, head_dim)
    value_new = value_flat.reshape(num_seqs, proposals, heads_local, head_dim)
    forget_cols = lax.dynamic_slice_in_dim(w_forget, tp_rank * heads_local, heads_local, 1)
    forget_bias = lax.dynamic_slice_in_dim(b_forget, tp_rank * heads_local, heads_local, 0)
    log_forget = jax.nn.log_sigmoid(
        jnp.dot(flat, forget_cols, preferred_element_type=jnp.float32) + forget_bias
    ).reshape(num_seqs, proposals, heads_local)
    ancestors = ancestry(parent, proposals)
    path = jnp.einsum("bij,bjh->bih", ancestors, log_forget, precision=lax.Precision.HIGHEST)
    valid = lengths + accepted
    positions = kv_rank * span + jnp.arange(span, dtype=jnp.int32)
    live = (positions[None, :] < valid[:, None])[:, None, None, :]
    score = (
        jnp.einsum("bihd,bkhd->bihk", query, key_cache, preferred_element_type=jnp.float32) * scale
        + path[..., None]
        - jnp.swapaxes(cum_cache, 1, 2)[:, None]
    )
    block_max = jnp.max(jnp.where(live, score, floor_value), axis=-1)
    weight = jnp.exp(jnp.where(live, score - block_max[..., None], floor_value))
    block_total = jnp.sum(weight, axis=-1)
    block_values = jnp.einsum(
        "bihk,bkhd->bihd",
        weight.astype(jnp.bfloat16),
        value_cache,
        preferred_element_type=jnp.float32,
    )
    owner = positions[None, :] == (valid - 1)[:, None]
    candidate = jnp.max(jnp.where(owner[:, :, None], cum_cache, floor_value), axis=1)
    tree_mask = (ancestors > 0.5)[:, :, None, :]
    tree_score = (
        jnp.einsum("bihd,bjhd->bihj", query, key_new, preferred_element_type=jnp.float32) * scale
        + path[..., None]
        - jnp.swapaxes(path, 1, 2)[:, None]
    )
    tree_max = jnp.max(jnp.where(tree_mask, tree_score, floor_value), axis=-1)
    tree_weight = jnp.exp(jnp.where(tree_mask, tree_score - tree_max[..., None], floor_value))
    tree_total = jnp.sum(tree_weight, axis=-1)
    tree_values = jnp.einsum(
        "bihj,bjhd->bihd",
        tree_weight.astype(jnp.bfloat16),
        value_new,
        preferred_element_type=jnp.float32,
    )
    tree_max_rows = tree_max.reshape(all_rows, heads_local)
    tree_total_rows = tree_total.reshape(all_rows, heads_local)
    tree_values_rows = tree_values.reshape(all_rows, heads_local, head_dim)
    cache_max, cache_total, cache_values, last_cum = merged(
        (block_max, block_total, block_values, candidate), "kv", combine_parts
    )
    last_rows = jnp.broadcast_to(last_cum[:, None, :], (num_seqs, proposals, heads_local)).reshape(
        all_rows, heads_local
    )
    attended = finish_rows(
        cache_max.reshape(all_rows, heads_local),
        cache_total.reshape(all_rows, heads_local),
        cache_values.reshape(all_rows, heads_local, head_dim),
        last_rows,
        tree_max_rows,
        tree_total_rows,
        tree_values_rows,
    )
    mixed_part = jnp.dot(attended, w_out, preferred_element_type=jnp.float32)
    mixed_sum = lax.psum_scatter(
        mixed_part.astype(jnp.bfloat16), "tp", scatter_dimension=1, tiled=True
    ).astype(jnp.float32)
    squares = lax.psum(jnp.sum(mixed_sum * mixed_sum, axis=1), ("kv", "tp"))
    mixed = (mixed_sum * lax.rsqrt(squares / model_width + epsilon)[:, None] * gain_post).astype(
        jnp.bfloat16
    )
    mixed = mixed.reshape(num_seqs, proposals, mixed_sum.shape[1])
    relative = positions[None, :] - valid[:, None]
    select = relative[:, :, None] == jnp.arange(proposals, dtype=jnp.int32)[None, None, :]
    written = (relative >= 0) & (relative < proposals)
    placed_keys = jnp.einsum(
        "bkj,bjhd->bkhd", select.astype(jnp.bfloat16), key_new, preferred_element_type=jnp.float32
    ).astype(jnp.bfloat16)
    placed_values = jnp.einsum(
        "bkj,bjhd->bkhd", select.astype(jnp.bfloat16), value_new, preferred_element_type=jnp.float32
    ).astype(jnp.bfloat16)
    key_out = jnp.where(written[:, :, None, None], placed_keys, key_cache)
    value_out = jnp.where(written[:, :, None, None], placed_values, value_cache)
    cum_new = last_cum[:, None, :] + path
    placed_cum = jnp.einsum(
        "bkj,bjh->bkh", select.astype(jnp.float32), cum_new, precision=lax.Precision.HIGHEST
    )
    cum_out = jnp.where(written[:, :, None], placed_cum, cum_cache)
    return (mixed, key_out, value_out, cum_out)


MESH = pl.DeviceIdType.MESH
HI = lax.Precision.HIGHEST
F32 = jnp.float32
BF = jnp.bfloat16


def iota(shape, dim):
    return lax.broadcasted_iota(jnp.int32, shape, dim)


def hot(mask):
    return jnp.where(mask, 1.0, 0.0).astype(F32)


def dot_hi(a, b, dims=(((1,), (0,)), ((), ()))):
    return lax.dot_general(a, b, dims, precision=HI, preferred_element_type=F32)


NT = (((1,), (1,)), ((), ()))


def layer_kernel(
    n,
    nt,
    num_seqs,
    prop,
    heads,
    hd,
    span,
    tok,
    gain,
    wq,
    wk,
    wv,
    wft,
    bias,
    wo,
    gpost,
    kc,
    vc,
    cum,
    lens,
    accs,
    parent,
    mixed_out,
    k_out,
    v_out,
    cum_out,
    tokv,
    normed,
    wv3,
    wov,
    kcv,
    vcv,
    part,
    rs_recv,
    qkv,
    st_send,
    val_send,
    st_recv,
    val_recv,
    cand_send,
    cand_recv,
    brow,
    anc,
    tpath,
    ptile,
    att,
    o_send,
    o_recv,
    sq_send,
    sq_recv,
    sq2_send,
    sq2_recv,
    loc,
    ssem,
    rsem,
    tssem,
    trsem,
):
    me = lax.axis_index("kv")
    mt = lax.axis_index("tp")
    rows = num_seqs * prop
    width = tok.shape[1]
    hw = heads * hd
    kdim = wq.shape[0]
    cols = heads * span
    sp = num_seqs // n
    R = sp * prop
    hp = heads * prop
    L = sp * hp
    scale = hd ** (-0.5)
    base = me * span
    heads_all = wft.shape[0]

    barrier = pltpu.get_barrier_semaphore()

    def greet(d, c):
        pl.semaphore_signal(
            barrier, inc=1, device_id={"kv": lax.rem(me + d, n)}, device_id_type=MESH
        )
        return c

    def greet_t(d, c):
        pl.semaphore_signal(
            barrier, inc=1, device_id={"tp": lax.rem(mt + d, nt)}, device_id_type=MESH
        )
        return c

    lax.fori_loop(1, n, greet, 0)
    lax.fori_loop(1, nt, greet_t, 0)

    in_tok = pltpu.make_async_copy(tok, tokv, loc.at[0])
    in_w = [pltpu.make_async_copy(w, wv3.at[i], loc.at[1 + i]) for i, w in enumerate((wq, wk, wv))]
    in_kc = pltpu.make_async_copy(kc, kcv, loc.at[4])
    in_vc = pltpu.make_async_copy(vc, vcv, loc.at[5])
    in_wo = pltpu.make_async_copy(wo, wov, loc.at[6])
    in_tok.start()
    for c in in_w:
        c.start()
    in_kc.start()
    in_vc.start()
    in_wo.start()

    def to_kv(ph, d, src, dst, sign=1):
        peer = lax.rem(me + sign * d + n, n)
        return pltpu.make_async_remote_copy(
            src_ref=src,
            dst_ref=dst,
            send_sem=ssem.at[ph, d],
            recv_sem=rsem.at[ph, d],
            device_id={"kv": peer},
            device_id_type=MESH,
        )

    def to_tp(ph, d, src, dst):
        peer = lax.rem(mt + d, nt)
        return pltpu.make_async_remote_copy(
            src_ref=src,
            dst_ref=dst,
            send_sem=tssem.at[ph, d],
            recv_sem=trsem.at[ph, d],
            device_id={"tp": peer},
            device_id_type=MESH,
        )

    def up(d):
        return lax.rem(me + d, n)

    def down(d):
        return lax.rem(me - d + n, n)

    def rrow(i):
        return pl.ds(pl.multiple_of(i * R, R), R)

    def rs_copy(ph, d):
        return to_kv(ph, d, part.at[ph, rrow(up(d))], rs_recv.at[ph, d])

    def ag_copy(ph, d):
        return to_kv(3 + ph, d, qkv.at[ph, rrow(me)], qkv.at[ph, rrow(me)])

    def ag_wait(ph, d):
        to_kv(3 + ph, d, qkv.at[ph, rrow(me)], qkv.at[ph, rrow(down(d))]).wait_recv()

    def stat_copy(d):
        return to_kv(6, d, st_send.at[d], st_recv.at[d], -1)

    def val_copy(d):
        return to_kv(7, d, val_send.at[d], val_recv.at[d], -1)

    def cand_copy(d):
        return to_kv(8, d, cand_send, cand_recv.at[d])

    def att_copy(d):
        return to_kv(9, d, att.at[rrow(me)], att.at[rrow(me)])

    def att_wait(d):
        to_kv(9, d, att.at[rrow(me)], att.at[rrow(down(d))]).wait_recv()

    def sq_copy(d):
        return to_kv(10, d, sq_send, sq_recv.at[d])

    def each(count, fn):
        def body(d, c):
            fn(d)
            return c

        lax.fori_loop(1, count, body, 0)

    in_tok.wait()
    nb = prop

    def norm_rows(i, c):
        sl = pl.ds(pl.multiple_of(i * nb, nb), nb)
        t = tokv[sl, :].astype(F32)
        inv = lax.rsqrt(jnp.mean(t * t, axis=-1, keepdims=True) + epsilon)
        normed[sl, :] = (t * inv * gain[...]).astype(BF)
        return c

    lax.fori_loop(0, rows // nb, norm_rows, 0)
    local = normed[:, pl.ds(pl.multiple_of(me * kdim, kdim), kdim)]
    pl.semaphore_wait(barrier, n - 1 + nt - 1)
    for ph in range(3):
        in_w[ph].wait()
        part[ph] = jnp.dot(local, wv3[ph], preferred_element_type=F32).astype(BF)
        each(n, lambda d: rs_copy(ph, d).start())

    r64 = num_seqs * heads
    c64 = cum[...]
    srow = iota((r64, span), 0) // heads
    lane = iota((r64, span), 1)
    rel64 = jnp.zeros((r64, span), jnp.int32)
    rel16 = jnp.zeros((num_seqs, cols), jnp.int32)
    s16 = iota((num_seqs, cols), 0)
    for s in range(num_seqs):
        rel_s = lens[s] + accs[s] - base
        rel64 = jnp.where(srow == s, rel_s, rel64)
        rel16 = jnp.where(s16 == s, rel_s, rel16)
    cand = jnp.max(jnp.where(lane == rel64 - 1, c64, floor_value), axis=1, keepdims=True)
    diag = iota((r64, 128), 0) == iota((r64, 128), 1)
    cand_lane = jnp.sum(jnp.where(diag, cand, 0.0), axis=0, keepdims=True)
    cand_send[...] = jnp.broadcast_to(cand_lane, (8, 128))
    each(n, lambda d: cand_copy(d).start())

    spread = hot(iota((span, cols), 1) // heads == iota((span, cols), 0))
    e1 = dot_hi(c64, spread)
    e1 = jnp.where(iota((r64, cols), 0) % heads == iota((r64, cols), 1) % heads, e1, 0.0)
    take = hot(iota((num_seqs, r64), 1) // heads == iota((num_seqs, r64), 0))
    cflat = dot_hi(take, e1)
    brow[...] = jnp.where(iota((num_seqs, cols), 1) // heads < rel16, -cflat, floor_value)

    ri = iota((rows, rows), 0)
    ci = iota((rows, rows), 1)
    pick = hot(iota((rows, num_seqs), 0) // prop == iota((rows, num_seqs), 1))
    pb = dot_hi(pick, parent[...].astype(F32))
    pcol = jnp.sum(
        jnp.where(iota((rows, prop), 1) == iota((rows, prop), 0) % prop, pb, 0.0),
        axis=1,
        keepdims=True,
    )
    target = jnp.where(pcol >= 0.0, (ri // prop * prop).astype(F32) + pcol, -1.0)
    a = jnp.where((ri == ci) | (ci.astype(F32) == target), 1.0, 0.0)
    for sweep in range(max(1, (prop - 1).bit_length())):
        low = a.astype(BF)
        a = jnp.minimum(jnp.dot(low, low, preferred_element_type=F32), 1.0)
    anc[...] = a
    lf = lax.dot_general(wft[...], normed[...], NT, preferred_element_type=F32)
    bcol = jnp.zeros((heads_all, rows), F32)
    for h in range(heads_all):
        bcol = jnp.where(iota((heads_all, rows), 0) == h, bias[h], bcol)
    z = lf + bcol
    lf = jnp.minimum(z, 0.0) - jnp.log1p(jnp.exp(-jnp.abs(z)))
    path_t = dot_hi(lf, a, NT)
    rep = hot(iota((r64, heads_all), 1) == mt * heads + iota((r64, heads_all), 0) % heads)
    pm = dot_hi(rep, path_t)
    pm = jnp.where(iota((r64, rows), 1) // prop == iota((r64, rows), 0) // heads, pm, 0.0)
    fold = hot(iota((rows, 128), 0) % prop == iota((rows, 128), 1) % prop)
    pt = dot_hi(pm, fold)
    ptile[...] = pt
    ptm = jnp.where((iota((r64, 128), 1) // prop) % heads == iota((r64, 128), 0) % heads, pt, 0.0)
    tpath[...] = dot_hi(take, ptm)

    def reduce_part(ph):
        total = part[ph, rrow(me)].astype(F32)
        for d in range(1, n):
            rs_copy(ph, d).wait_recv()
            total = total + rs_recv[ph, d].astype(F32)
        qkv[ph, rrow(me)] = total.astype(BF)
        each(n, lambda d: ag_copy(ph, d).start())

    for ph in range(3):
        reduce_part(ph)

    in_kc.wait()
    in_vc.wait()
    same_head = iota((hp, cols), 0) // prop == iota((hp, cols), 1) % heads
    diag_l = iota((L, L), 0) == iota((L, L), 1)

    def heads_of(ph, s):
        block = qkv[ph, pl.ds(pl.multiple_of(s * prop, prop), prop), :]
        return jnp.concatenate([block[:, h * hd : (h + 1) * hd] for h in range(heads)], axis=0)

    def block_part(src):
        maxes, totals, values = [], [], []
        for j in range(sp):
            s = src * sp + j
            q = heads_of(0, s)
            sc = lax.dot_general(q, kcv[s], NT, preferred_element_type=F32) * scale
            sc = jnp.where(same_head, sc + brow[pl.ds(s, 1), :], floor_value)
            m = jnp.max(sc, axis=1, keepdims=True)
            w = jnp.exp(sc - m)
            maxes.append(m)
            totals.append(jnp.sum(w, axis=1, keepdims=True))
            values.append(
                jnp.dot(w.astype(BF), vcv[s], preferred_element_type=F32).astype(BF)
            )
        m = jnp.concatenate(maxes, axis=0)
        t = jnp.concatenate(totals, axis=0)
        m_lane = jnp.sum(jnp.where(diag_l, m, 0.0), axis=0, keepdims=True)
        t_lane = jnp.sum(jnp.where(diag_l, t, 0.0), axis=0, keepdims=True)
        stats = jnp.where(iota((8, L), 0) == 0, m_lane, t_lane)
        return stats, jnp.concatenate(values, axis=0)

    def remote_block(d):
        ag_wait(0, d)
        stats, values = block_part(down(d))
        st_send[d] = stats
        val_send[d] = values
        stat_copy(d).start()
        val_copy(d).start()

    each(n, remote_block)
    stats, values = block_part(me)
    st_recv[0] = stats
    val_recv[0] = values

    fold_h = iota((rows, hp), 0)
    tmax, ttot, tval = [], [], []
    for j in range(sp):
        s = me * sp + j
        q = heads_of(0, s)
        k = heads_of(1, s)
        v = heads_of(2, s)
        arows = anc[pl.ds(pl.multiple_of(s * prop, prop), prop), :]
        sel = hot(fold_h == s * prop + iota((rows, hp), 1) % prop).astype(BF)
        am = jnp.dot(arows.astype(BF), sel, preferred_element_type=F32)
        am = jnp.concatenate([am] * heads, axis=0)
        mask = (am > 0.5) & (iota((hp, hp), 0) // prop == iota((hp, hp), 1) // prop)
        sc = lax.dot_general(q, k, NT, preferred_element_type=F32) * scale
        sc = jnp.where(mask, sc - tpath[pl.ds(s, 1), 0:hp], floor_value)
        m = jnp.max(sc, axis=1, keepdims=True)
        w = jnp.where(mask, jnp.exp(sc - m), 0.0)
        tmax.append(m)
        ttot.append(jnp.sum(w, axis=1, keepdims=True))
        tval.append(jnp.dot(w.astype(BF), v, preferred_element_type=F32))
    tree_max = jnp.concatenate(tmax, axis=0)
    tree_tot = jnp.concatenate(ttot, axis=0)
    tree_val = jnp.concatenate(tval, axis=0)

    last_lane = cand_send[...]
    for d in range(1, n):
        cand_copy(d).wait_recv()
        last_lane = jnp.maximum(last_lane, cand_recv[d])
    last_col = jnp.sum(jnp.where(diag, last_lane[0:1], 0.0), axis=1, keepdims=True)
    own_rows = iota((L, 128), 0)
    own_pick = iota((L, 128), 1) == (me * sp + own_rows // hp) * heads + (own_rows % hp) // prop
    last_own = jnp.sum(jnp.where(own_pick, last_lane[0:1], 0.0), axis=1, keepdims=True)

    shifted_path = ptile[...]
    for b in range((span - 1).bit_length()):
        moved = pltpu.roll(shifted_path, 1 << b, 1)
        shifted_path = jnp.where((rel64 >> b) & 1 == 1, moved, shifted_path)
    off = lane - rel64
    cum_out[...] = jnp.where((off >= 0) & (off < prop), last_col + shifted_path, cum[...])

    for d in range(1, n):
        stat_copy(d).wait_recv()
    top = st_recv[0]
    for d in range(1, n):
        top = jnp.maximum(top, st_recv[d])
    top = top[0:1]

    def col(x):
        return jnp.sum(jnp.where(diag_l, x, 0.0), axis=1, keepdims=True)

    cache_tot = jnp.zeros((1, L), F32)
    scales = []
    for d in range(n):
        sd = jnp.exp(st_recv[d, 0:1] - top)
        scales.append(col(sd))
        cache_tot = cache_tot + st_recv[d, 1:2] * sd
    shifted = col(top) + last_own
    both = jnp.maximum(shifted, tree_max)
    cscale = jnp.exp(shifted - both)
    tscale = jnp.exp(tree_max - both)
    denom = col(cache_tot) * cscale + tree_tot * tscale
    vals = jnp.zeros((L, hd), F32)
    for d in range(n):
        if d > 0:
            val_copy(d).wait_recv()
        vals = vals + val_recv[d].astype(F32) * scales[d]
    attended = ((vals * cscale + tree_val * tscale) / denom).astype(BF)
    for j in range(sp):
        for h in range(heads):
            att[pl.ds(pl.multiple_of(me * R + j * prop, prop), prop), h * hd : (h + 1) * hd] = (
                attended[j * hp + h * prop : j * hp + (h + 1) * prop]
            )
    each(n, lambda d: att_copy(d).start())
    each(n, lambda d: ag_wait(1, d))
    each(n, lambda d: ag_wait(2, d))
    out_k = pltpu.make_async_copy(qkv.at[1], k_out, loc.at[7])
    out_v = pltpu.make_async_copy(qkv.at[2], v_out, loc.at[8])
    out_k.start()
    out_v.start()
    in_wo.wait()
    each(n, att_wait)
    full = jnp.dot(att[...], wov[...], preferred_element_type=F32).astype(BF)
    oc = o_send.shape[2]
    for t in range(nt):
        o_send[t] = full[:, t * oc : (t + 1) * oc]

    def o_copy(d):
        return to_tp(0, d, o_send.at[lax.rem(mt + d, nt)], o_recv.at[d])

    def sq2_copy(d):
        return to_tp(1, d, sq2_send, sq2_recv.at[d])

    each(nt, lambda d: o_copy(d).start())
    mixed = o_send[mt].astype(F32)
    for d in range(1, nt):
        o_copy(d).wait_recv()
        mixed = mixed + o_recv[d].astype(F32)
    sq_send[...] = dot_hi(jnp.ones((8, oc), F32), mixed * mixed, NT)
    each(n, lambda d: sq_copy(d).start())
    sq = sq_send[...]
    for d in range(1, n):
        sq_copy(d).wait_recv()
        sq = sq + sq_recv[d]
    sq2_send[...] = sq
    each(nt, lambda d: sq2_copy(d).start())
    for d in range(1, nt):
        sq2_copy(d).wait_recv()
        sq = sq + sq2_recv[d]
    ssum = dot_hi(sq, jnp.full((8, oc), 0.125, F32), (((0,), (0,)), ((), ())))
    mixed_out[...] = (mixed * lax.rsqrt(ssum / width + epsilon) * gpost[...]).astype(BF)

    def drain(d):
        for ph in range(3):
            rs_copy(ph, d).wait_send()
            ag_copy(ph, d).wait_send()
        stat_copy(d).wait_send()
        val_copy(d).wait_send()
        cand_copy(d).wait_send()
        att_copy(d).wait_send()
        sq_copy(d).wait_send()

    each(n, drain)

    def drain_t(d):
        o_copy(d).wait_send()
        sq2_copy(d).wait_send()

    each(nt, drain_t)
    out_k.wait()
    out_v.wait()


def write_kernel(num_seqs, prop, heads, hd, span, kc, vc, kn, vn, lens, accs, k_out, v_out, buf, sin, sout):
    base = lax.axis_index("kv") * span
    hp = heads * prop
    cols = heads * span
    win = hp + 16
    srcs, dsts, news = (kc, vc), (k_out, v_out), (kn, vn)
    for s in range(num_seqs):
        for i in range(2):
            pltpu.make_async_copy(srcs[i].at[s], buf.at[i, s], sin.at[i, s]).start()
    m = iota((win, hp), 1)
    diff = iota((win, hp), 0) - (m % prop * heads + m // prop)
    edge = iota((win, hd), 0)
    for s in range(num_seqs):
        first = (lens[s] + accs[s] - base) * heads
        start = pl.multiple_of(jnp.clip(first // 16 * 16, 0, cols - win), 16)
        sel = hot(diff == first - start).astype(BF)
        here = edge - (first - start)
        inside = (here >= 0) & (here < hp)
        for i in range(2):
            new = news[i][s * prop : (s + 1) * prop, :]
            new = jnp.concatenate([new[:, h * hd : (h + 1) * hd] for h in range(heads)], axis=0)
            placed = jnp.dot(sel, new, preferred_element_type=F32)
            pltpu.make_async_copy(srcs[i].at[s], buf.at[i, s], sin.at[i, s]).wait()
            old = buf[i, s, pl.ds(start, win), :].astype(F32)
            buf[i, s, pl.ds(start, win), :] = jnp.where(inside, placed, old).astype(BF)
            pltpu.make_async_copy(buf.at[i, s], dsts[i].at[s], sout.at[i, s]).start()
    for s in range(num_seqs):
        for i in range(2):
            pltpu.make_async_copy(buf.at[i, s], dsts[i].at[s], sout.at[i, s]).wait()


def fast_device(
    n,
    nt,
    tokens,
    gain_pre,
    w_query,
    w_key,
    w_value,
    w_forget,
    b_forget,
    w_out,
    gain_post,
    key_cache,
    value_cache,
    cum_cache,
    lengths,
    accepted,
    parent,
):
    num_seqs, prop, width = tokens.shape
    span, heads, hd = key_cache.shape[1:]
    rows = num_seqs * prop
    hw = heads * hd
    cols = heads * span
    sp = num_seqs // n
    R = sp * prop
    L = sp * heads * prop
    oc = gain_post.shape[0]
    kc = key_cache.reshape(num_seqs, cols, hd)
    vc = value_cache.reshape(num_seqs, cols, hd)
    cum = jnp.swapaxes(cum_cache, 1, 2).reshape(num_seqs * heads, span)
    anyspec = pl.BlockSpec(memory_space=pl.ANY)
    vmem = pl.BlockSpec(memory_space=pltpu.VMEM)
    smem = pl.BlockSpec(memory_space=pltpu.SMEM)
    V = pltpu.VMEM
    D = pltpu.SemaphoreType.DMA
    mixed, k_new, v_new, cum_new = pl.pallas_call(
        functools.partial(layer_kernel, n, nt, num_seqs, prop, heads, hd, span),
        out_shape=(
            jax.ShapeDtypeStruct((rows, oc), BF),
            jax.ShapeDtypeStruct((rows, hw), BF),
            jax.ShapeDtypeStruct((rows, hw), BF),
            jax.ShapeDtypeStruct(cum.shape, F32),
        ),
        in_specs=[
            anyspec,
            vmem,
            anyspec,
            anyspec,
            anyspec,
            vmem,
            smem,
            anyspec,
            vmem,
            anyspec,
            anyspec,
            vmem,
            smem,
            smem,
            vmem,
        ],
        out_specs=(vmem, anyspec, anyspec, vmem),
        scratch_shapes=[
            V((rows, width), BF),
            V((rows, width), BF),
            V((3,) + w_query.shape, BF),
            V(w_out.shape, BF),
            V(kc.shape, BF),
            V(vc.shape, BF),
            V((3, rows, hw), BF),
            V((3, n, R, hw), BF),
            V((3, rows, hw), BF),
            V((n, 8, L), F32),
            V((n, L, hd), BF),
            V((n, 8, L), F32),
            V((n, L, hd), BF),
            V((8, 128), F32),
            V((n, 8, 128), F32),
            V((num_seqs, cols), F32),
            V((rows, rows), F32),
            V((num_seqs, 128), F32),
            V((num_seqs * heads, 128), F32),
            V((rows, hw), BF),
            V((nt, rows, oc), BF),
            V((nt, rows, oc), BF),
            V((8, rows), F32),
            V((n, 8, rows), F32),
            V((8, rows), F32),
            V((nt, 8, rows), F32),
            D((9,)),
            D((11, n)),
            D((11, n)),
            D((2, nt)),
            D((2, nt)),
        ],
        compiler_params=pltpu.CompilerParams(
            collective_id=0, has_side_effects=True, vmem_limit_bytes=50 * 1024 * 1024
        ),
        name="layer",
    )(
        tokens.reshape(rows, width),
        gain_pre.reshape(1, width),
        w_query,
        w_key,
        w_value,
        w_forget.T,
        b_forget,
        w_out,
        gain_post.reshape(1, oc),
        kc,
        vc,
        cum,
        lengths,
        accepted,
        parent,
    )
    key_out, value_out = pl.pallas_call(
        functools.partial(write_kernel, num_seqs, prop, heads, hd, span),
        out_shape=(
            jax.ShapeDtypeStruct(kc.shape, BF),
            jax.ShapeDtypeStruct(vc.shape, BF),
        ),
        in_specs=[anyspec, anyspec, vmem, vmem, smem, smem],
        out_specs=(anyspec, anyspec),
        scratch_shapes=[
            V((2,) + kc.shape, BF),
            D((2, num_seqs)),
            D((2, num_seqs)),
        ],
        compiler_params=pltpu.CompilerParams(vmem_limit_bytes=16 * 1024 * 1024),
        name="cache_write",
    )(kc, vc, k_new, v_new, lengths, accepted)
    cum_out = jnp.swapaxes(cum_new.reshape(num_seqs, heads, span), 1, 2)
    return (
        mixed.reshape(num_seqs, prop, oc),
        key_out.reshape(key_cache.shape),
        value_out.reshape(value_cache.shape),
        cum_out,
    )


def choose(mesh):
    n, nt = mesh.shape["kv"], mesh.shape["tp"]

    def body(*args):
        tokens, key_cache = args[0], args[9]
        num_seqs, prop = tokens.shape[:2]
        span, heads = key_cache.shape[1:3]
        fits = (
            num_seqs % n == 0
            and (num_seqs // n) * heads * prop == 128
            and span == 128
            and num_seqs * heads <= 128
            and prop % 16 == 0
        )
        if fits:
            return fast_device(n, nt, *args)
        return per_device(*args)

    return body


def solution(mesh):
    return jax.shard_map(
        choose(mesh),
        mesh=mesh,
        in_specs=(
            P(),
            P(),
            P("kv", "tp"),
            P("kv", "tp"),
            P("kv", "tp"),
            P(),
            P(),
            P("tp", "kv"),
            P(("kv", "tp")),
            P(None, "kv", "tp", None),
            P(None, "kv", "tp", None),
            P(None, "kv", "tp"),
            P(),
            P(),
            P(),
        ),
        out_specs=(
            P(None, None, ("kv", "tp")),
            P(None, "kv", "tp", None),
            P(None, "kv", "tp", None),
            P(None, "kv", "tp"),
        ),
        check_vma=False,
    )
```

profile of v0, /device:TPU:0, one launch (start us, length us, event | category | flops | bytes accessed | tf_op | source)
XLA Modules:
  0.0 97.8 jit_solution(13078138955926832517)
XLA Ops:
  0.6 0.0 copy-start.2
  0.6 1.0 %copy-done.2 = bf16[512,512]{1,0:T(8,128)(2,1)S(1)} copy-done((bf16[512,512]{1,0:T(8,128)(2,1)S(1)}, bf16[512,512]{1,0:T(8,128)(2,1)}, u32[]{:S(2)}) %copy-start.2) | copy-done | bytes 524312
  1.7 0.0 copy-start.3
  1.7 1.0 %copy-done.3 = bf16[512,512]{1,0:T(8,128)(2,1)S(1)} copy-done((bf16[512,512]{1,0:T(8,128)(2,1)S(1)}, bf16[512,512]{1,0:T(8,128)(2,1)}, u32[]{:S(2)}) %copy-start.3) | copy-done | bytes 524312
  2.7 0.0 copy-start.4
  2.7 1.0 %copy-done.4 = bf16[512,512]{1,0:T(8,128)(2,1)S(1)} copy-done((bf16[512,512]{1,0:T(8,128)(2,1)S(1)}, bf16[512,512]{1,0:T(8,128)(2,1)}, u32[]{:S(2)}) %copy-start.4) | copy-done | bytes 524312
  3.8 0.0 copy-start.5
  3.8 1.0 %copy-done.5 = bf16[512,512]{1,0:T(8,128)(2,1)S(1)} copy-done((bf16[512,512]{1,0:T(8,128)(2,1)S(1)}, bf16[512,512]{1,0:T(8,128)(2,1)}, u32[]{:S(2)}) %copy-start.5) | copy-done | bytes 524312
  4.8 0.0 copy-start.6
  4.8 0.9 copy-done.6
  5.7 0.0 copy-start.7
  5.7 0.8 copy-done.7
  6.5 0.0 copy-start.8
  6.5 0.7 copy-done.8
  7.2 0.0 copy-start.9
  7.2 0.7 copy-done.9
  7.9 0.0 copy-start.10
  7.9 0.7 copy-done.10
  8.5 0.0 copy-start.11
  8.5 0.7 copy-done.11
  9.2 0.0 copy-start.12
  9.2 0.7 copy-done.12
  9.9 0.0 copy-start.13
  9.9 0.7 copy-done.13
  10.5 0.0 copy-start
  10.5 0.0 copy-start.1
  10.5 74.2 %layer.1 = (bf16[256,128]{1,0:T(8,128)(2,1)S(1)}, bf16[256,512]{1,0:T(8,128)(2,1)S(1)}, bf16[256,512]{1,0:T(8,128)(2,1)S(1)}, f32[64,128]{1,0:T(8,128)S(1)}) custom-call(bf16[256,4096]{1,0:T(8,128)(2,1)} %bitcast.25, f32[1,4096]{1,0:T(1,128)S(1)} %bitcast.23, bf16[512,512]{1,0:T(8,128)(2,1)S(1)} %copy-done.2, bf16[512,512]{1,0:T(8,128)(2,1)S(1)} %copy-done.3, ...), custom_call_target="tpu_custom_call" | custom-call | tf_op jit(solution)/shard_map/layer/pallas_call | solution.py:711
  84.7 0.0 copy-done
  84.7 0.0 copy-done.1
  84.7 11.8 %cache_write.1 = (bf16[16,512,128]{2,1,0:T(8,128)(2,1)}, bf16[16,512,128]{2,1,0:T(8,128)(2,1)}) custom-call(bf16[16,512,128]{2,1,0:T(8,128)(2,1)S(1)} %bitcast.16, bf16[16,512,128]{2,1,0:T(8,128)(2,1)S(1)} %bitcast.18, bf16[256,512]{1,0:T(8,128)(2,1)S(1)} %get-tuple-element.11.kn, bf16[256,512]{1,0:T(8,128)(2,1)S(1)} %get-tuple-element.12.vn, ...), custom_call_target="tpu_custom_call" | custom-call | tf_op jit(solution)/shard_map/cache_write/pallas_call | solution.py:791
  96.5 0.6 copy.21
  97.1 0.6 copy.22
Async XLA Ops:
  0.6 1.0 %copy-start.2 = (bf16[512,512]{1,0:T(8,128)(2,1)S(1)}, bf16[512,512]{1,0:T(8,128)(2,1)}, u32[]{:S(2)}) copy-start(bf16[512,512]{1,0:T(8,128)(2,1)} %wq.1) | copy-start | bytes 1572868
  1.7 1.0 %copy-start.3 = (bf16[512,512]{1,0:T(8,128)(2,1)S(1)}, bf16[512,512]{1,0:T(8,128)(2,1)}, u32[]{:S(2)}) copy-start(bf16[512,512]{1,0:T(8,128)(2,1)} %wk.1) | copy-start | bytes 1572868
  2.7 1.0 %copy-start.4 = (bf16[512,512]{1,0:T(8,128)(2,1)S(1)}, bf16[512,512]{1,0:T(8,128)(2,1)}, u32[]{:S(2)}) copy-start(bf16[512,512]{1,0:T(8,128)(2,1)} %wv.1) | copy-start | bytes 1572868
  3.8 1.0 %copy-start.5 = (bf16[512,512]{1,0:T(8,128)(2,1)S(1)}, bf16[512,512]{1,0:T(8,128)(2,1)}, u32[]{:S(2)}) copy-start(bf16[512,512]{1,0:T(8,128)(2,1)} %wo.1) | copy-start | bytes 1572868
  4.8 0.9 copy-start.6
  5.7 0.8 copy-start.7
  6.5 0.7 copy-start.8
  7.2 0.7 copy-start.9
  7.9 0.7 copy-start.10
  8.5 0.7 copy-start.11
  9.2 0.7 copy-start.12
  9.9 0.7 copy-start.13
  10.5 74.2 %copy-start = (bf16[16,128,4,128]{3,2,1,0:T(4,128)(2,1)S(1)}, bf16[16,128,4,128]{3,2,1,0:T(4,128)(2,1)}, u32[]{:S(2)}) copy-start(bf16[16,128,4,128]{3,2,1,0:T(4,128)(2,1)} %param.24) | copy-start | bytes 6291460
  10.5 74.2 %copy-start.1 = (bf16[16,128,4,128]{3,2,1,0:T(4,128)(2,1)S(1)}, bf16[16,128,4,128]{3,2,1,0:T(4,128)(2,1)}, u32[]{:S(2)}) copy-start(bf16[16,128,4,128]{3,2,1,0:T(4,128)(2,1)} %param.25) | copy-start | bytes 6291460
where the time goes:
time: 98.3 us; the launch traced here: 97.8 us
  Pallas kernels  86 us (87%)
  local copies, waits for them, and re-layouts  11.1 us (11%)
    pallas_call x1, Pallas kernels, fast_device(): pl.pallas_call(functools.partial(layer_kernel, n, nt, num_seqs, prop, hea...  74.2 us
    pallas_call x1, Pallas kernels, fast_device(): pl.pallas_call(functools.partial(write_kernel, num_seqs, prop, heads, hd,...  11.8 us
    unnamed x30, local copies, waits for them, and re-layouts  11.1 us

commit v1 on v0

--- a/solution.py
+++ b/solution.py
@@ -215,6 +215,15 @@
 NT = (((1,), (1,)), ((), ()))
 
 
+def flip(value, mask):
+    total = 0
+    bit = 1
+    while bit < 64:
+        total = total + ((value // bit + mask // bit) % 2) * bit
+        bit *= 2
+    return total
+
+
 def layer_kernel(
     n,
     nt,
@@ -223,34 +232,49 @@
     heads,
     hd,
     span,
-    tok,
+    tok_h,
+    gain_h,
+    wq_h,
+    wk_h,
+    wv_h,
+    wft_h,
+    bias_h,
+    wo_h,
+    gpost_h,
+    kc_h,
+    vc_h,
+    cum_h,
+    lens_h,
+    accs_h,
+    parent_h,
+    mixed_out,
+    cum_out,
+    knew_out,
+    vnew_out,
+    tokv,
     gain,
-    wq,
-    wk,
-    wv,
+    wqkv,
     wft,
     bias,
-    wo,
+    wov,
     gpost,
-    kc,
-    vc,
+    kcv,
+    vcv,
     cum,
     lens,
     accs,
     parent,
-    mixed_out,
-    k_out,
-    v_out,
-    cum_out,
-    tokv,
-    normed,
-    wv3,
-    wov,
-    kcv,
-    vcv,
-    part,
-    rs_recv,
-    qkv,
+    ssq,
+    invv,
+    xloc,
+    part_q,
+    q_recv,
+    q_full,
+    part_kv,
+    kv_y,
+    kv_zs,
+    kv_zr,
+    kv_full,
     st_send,
     val_send,
     st_recv,
@@ -266,20 +290,19 @@
     o_recv,
     sq_send,
     sq_recv,
-    sq2_send,
-    sq2_recv,
     loc,
     ssem,
     rsem,
     tssem,
     trsem,
+    qssem,
+    qrsem,
 ):
     me = lax.axis_index("kv")
     mt = lax.axis_index("tp")
-    rows = num_seqs * prop
-    width = tok.shape[1]
+    rows, width = tokv.shape
     hw = heads * hd
-    kdim = wq.shape[0]
+    kdim = wq_h.shape[0]
     cols = heads * span
     sp = num_seqs // n
     R = sp * prop
@@ -288,93 +311,111 @@
     scale = hd ** (-0.5)
     base = me * span
     heads_all = wft.shape[0]
+    half = n // 2
+    everyone = n * nt
 
     barrier = pltpu.get_barrier_semaphore()
 
-    def greet(d, c):
+    def greet(e, c):
         pl.semaphore_signal(
-            barrier, inc=1, device_id={"kv": lax.rem(me + d, n)}, device_id_type=MESH
+            barrier,
+            inc=1,
+            device_id={"kv": flip(me, e // nt), "tp": flip(mt, e % nt)},
+            device_id_type=MESH,
         )
         return c
 
-    def greet_t(d, c):
-        pl.semaphore_signal(
-            barrier, inc=1, device_id={"tp": lax.rem(mt + d, nt)}, device_id_type=MESH
+    chunks = 4
+    crow = rows // chunks
+    in_tok = [
+        pltpu.make_async_copy(
+            tok_h.at[pl.ds(i * crow, crow)], tokv.at[pl.ds(i * crow, crow)], loc.at[i]
         )
-        return c
-
-    lax.fori_loop(1, n, greet, 0)
-    lax.fori_loop(1, nt, greet_t, 0)
-
-    in_tok = pltpu.make_async_copy(tok, tokv, loc.at[0])
-    in_w = [pltpu.make_async_copy(w, wv3.at[i], loc.at[1 + i]) for i, w in enumerate((wq, wk, wv))]
-    in_kc = pltpu.make_async_copy(kc, kcv, loc.at[4])
-    in_vc = pltpu.make_async_copy(vc, vcv, loc.at[5])
-    in_wo = pltpu.make_async_copy(wo, wov, loc.at[6])
-    in_tok.start()
-    for c in in_w:
+        for i in range(chunks)
+    ]
+    later = [
+        (gain_h, gain),
+        (wq_h, wqkv.at[0]),
+        (wk_h, wqkv.at[1]),
+        (wv_h, wqkv.at[2]),
+        (wft_h, wft),
+        (bias_h, bias),
+        (lens_h, lens),
+        (accs_h, accs),
+        (parent_h, parent),
+        (cum_h, cum),
+        (gpost_h, gpost),
+        (kc_h, kcv),
+        (vc_h, vcv),
+        (wo_h, wov),
+    ]
+    copies = [
+        pltpu.make_async_copy(src, dst, loc.at[chunks + i]) for i, (src, dst) in enumerate(later)
+    ]
+    (
+        in_gain,
+        in_wq,
+        in_wk,
+        in_wv,
+        in_wft,
+        in_bias,
+        in_lens,
+        in_accs,
+        in_parent,
+        in_cum,
+        in_gpost,
+        in_kc,
+        in_vc,
+        in_wo,
+    ) = copies
+    for c in in_tok:
         c.start()
-    in_kc.start()
-    in_vc.start()
-    in_wo.start()
-
-    def to_kv(ph, d, src, dst, sign=1):
-        peer = lax.rem(me + sign * d + n, n)
+    for c in copies:
+        c.start()
+    lax.fori_loop(1, everyone, greet, 0)
+
+    def to_kv(ph, slot, mask, src, dst):
         return pltpu.make_async_remote_copy(
             src_ref=src,
             dst_ref=dst,
-            send_sem=ssem.at[ph, d],
-            recv_sem=rsem.at[ph, d],
-            device_id={"kv": peer},
+            send_sem=ssem.at[ph, slot],
+            recv_sem=rsem.at[ph, slot],
+            device_id={"kv": flip(me, mask)},
             device_id_type=MESH,
         )
 
-    def to_tp(ph, d, src, dst):
-        peer = lax.rem(mt + d, nt)
-        return pltpu.make_async_remote_copy(
-            src_ref=src,
-            dst_ref=dst,
-            send_sem=tssem.at[ph, d],
-            recv_sem=trsem.at[ph, d],
-            device_id={"tp": peer},
-            device_id_type=MESH,
-        )
-
-    def up(d):
-        return lax.rem(me + d, n)
-
-    def down(d):
-        return lax.rem(me - d + n, n)
-
     def rrow(i):
         return pl.ds(pl.multiple_of(i * R, R), R)
 
-    def rs_copy(ph, d):
-        return to_kv(ph, d, part.at[ph, rrow(up(d))], rs_recv.at[ph, d])
-
-    def ag_copy(ph, d):
-        return to_kv(3 + ph, d, qkv.at[ph, rrow(me)], qkv.at[ph, rrow(me)])
-
-    def ag_wait(ph, d):
-        to_kv(3 + ph, d, qkv.at[ph, rrow(me)], qkv.at[ph, rrow(down(d))]).wait_recv()
-
-    def stat_copy(d):
-        return to_kv(6, d, st_send.at[d], st_recv.at[d], -1)
-
-    def val_copy(d):
-        return to_kv(7, d, val_send.at[d], val_recv.at[d], -1)
-
-    def cand_copy(d):
-        return to_kv(8, d, cand_send, cand_recv.at[d])
-
-    def att_copy(d):
-        return to_kv(9, d, att.at[rrow(me)], att.at[rrow(me)])
-
-    def att_wait(d):
-        to_kv(9, d, att.at[rrow(me)], att.at[rrow(down(d))]).wait_recv()
-
-    def sq_copy(d):
-        return to_kv(10, d, sq_send, sq_recv.at[d])
+    def q_rs(m):
+        return to_kv(0, m, m, part_q.at[rrow(flip(me, m))], q_recv.at[m])
+
+    def q_ag(m):
+        return to_kv(1, m, m, q_full.at[rrow(me)], q_full.at[rrow(me)])
+
+    def kv_yrs(m):
+        return to_kv(2, m, 1, part_kv.at[rrow(flip(me, m + 1))], kv_y.at[m // 2])
+
+    def kv_zrs(m):
+        return to_kv(2, m + 1, m, kv_zs.at[m // 2], kv_zr.at[m // 2])
+
+    def cand_copy(m):
+        return to_kv(3, m, m, cand_send, cand_recv.at[m])
+
+    def stat_copy(m):
+        return to_kv(4, m, m, st_send.at[m], st_recv.at[m])
+
+    def val_copy(m):
+        return to_kv(5, m, m, val_send.at[m], val_recv.at[m])
+
+    def att_copy(m):
+        return to_kv(6, m, m, att.at[rrow(me)], att.at[rrow(me)])
+
+    def kv_zag(m):
+        return to_kv(7, m, m, kv_full.at[rrow(me)], kv_full.at[rrow(me)])
+
+    def kv_yag(m):
+        return to_kv(7, m + 1, 1, kv_full.at[rrow(flip(me, m))], kv_full.at[rrow(flip(me, m))])
 
     def each(count, fn):
         def body(d, c):
@@ -383,24 +424,49 @@
 
         lax.fori_loop(1, count, body, 0)
 
-    in_tok.wait()
+    def each_far(count, fn):
+        each(count, lambda d: fn(count - d))
+
+    zmasks = list(range(2, n, 2))
     nb = prop
-
-    def norm_rows(i, c):
+    lanes = 128
+
+    def sum_rows(i, c):
         sl = pl.ds(pl.multiple_of(i * nb, nb), nb)
-        t = tokv[sl, :].astype(F32)
-        inv = lax.rsqrt(jnp.mean(t * t, axis=-1, keepdims=True) + epsilon)
-        normed[sl, :] = (t * inv * gain[...]).astype(BF)
+        accs4 = [None] * 4
+        for j in range(width // lanes):
+            t = tokv[sl, j * lanes : (j + 1) * lanes].astype(F32)
+            p = t * t
+            accs4[j % 4] = p if accs4[j % 4] is None else accs4[j % 4] + p
+        ssq[sl, :] = (accs4[0] + accs4[1]) + (accs4[2] + accs4[3])
         return c
 
-    lax.fori_loop(0, rows // nb, norm_rows, 0)
-    local = normed[:, pl.ds(pl.multiple_of(me * kdim, kdim), kdim)]
-    pl.semaphore_wait(barrier, n - 1 + nt - 1)
-    for ph in range(3):
-        in_w[ph].wait()
-        part[ph] = jnp.dot(local, wv3[ph], preferred_element_type=F32).astype(BF)
-        each(n, lambda d: rs_copy(ph, d).start())
-
+    for i in range(chunks):
+        in_tok[i].wait()
+        lax.fori_loop(i * crow // nb, (i + 1) * crow // nb, sum_rows, 0)
+    total = dot_hi(ssq[...], jnp.ones((lanes, lanes), F32))
+    inv = lax.rsqrt(total / width + epsilon)
+    invv[...] = inv
+    in_gain.wait()
+    for j in range(kdim // lanes):
+        at = pl.ds(pl.multiple_of(me * kdim + j * lanes, lanes), lanes)
+        xloc[:, j * lanes : (j + 1) * lanes] = (
+            tokv[:, at].astype(F32) * inv * gain[:, at]
+        ).astype(BF)
+    in_wq.wait()
+    part_q[...] = jnp.dot(xloc[...], wqkv[0], preferred_element_type=F32).astype(BF)
+    pl.semaphore_wait(barrier, everyone - 1)
+    each_far(n, lambda m: q_rs(m).start())
+    in_wk.wait()
+    in_wv.wait()
+    part_kv[:, 0:hw] = jnp.dot(xloc[...], wqkv[1], preferred_element_type=F32).astype(BF)
+    part_kv[:, hw : 2 * hw] = jnp.dot(xloc[...], wqkv[2], preferred_element_type=F32).astype(BF)
+    for m in zmasks[::-1] + [0]:
+        kv_yrs(m).start()
+
+    in_lens.wait()
+    in_accs.wait()
+    in_cum.wait()
     r64 = num_seqs * heads
     c64 = cum[...]
     srow = iota((r64, span), 0) // heads
@@ -414,9 +480,8 @@
         rel16 = jnp.where(s16 == s, rel_s, rel16)
     cand = jnp.max(jnp.where(lane == rel64 - 1, c64, floor_value), axis=1, keepdims=True)
     diag = iota((r64, 128), 0) == iota((r64, 128), 1)
-    cand_lane = jnp.sum(jnp.where(diag, cand, 0.0), axis=0, keepdims=True)
-    cand_send[...] = jnp.broadcast_to(cand_lane, (8, 128))
-    each(n, lambda d: cand_copy(d).start())
+    cand_send[...] = jnp.sum(jnp.where(diag, cand, 0.0), axis=0, keepdims=True)
+    each_far(n, lambda m: cand_copy(m).start())
 
     spread = hot(iota((span, cols), 1) // heads == iota((span, cols), 0))
     e1 = dot_hi(c64, spread)
@@ -425,6 +490,7 @@
     cflat = dot_hi(take, e1)
     brow[...] = jnp.where(iota((num_seqs, cols), 1) // heads < rel16, -cflat, floor_value)
 
+    in_parent.wait()
     ri = iota((rows, rows), 0)
     ci = iota((rows, rows), 1)
     pick = hot(iota((rows, num_seqs), 0) // prop == iota((rows, num_seqs), 1))
@@ -440,11 +506,20 @@
         low = a.astype(BF)
         a = jnp.minimum(jnp.dot(low, low, preferred_element_type=F32), 1.0)
     anc[...] = a
-    lf = lax.dot_general(wft[...], normed[...], NT, preferred_element_type=F32)
+    in_wft.wait()
+    in_bias.wait()
+    wscaled = wft[...].astype(F32) * gain[...]
+    whigh = wscaled.astype(BF)
+    wlow = (wscaled - whigh.astype(F32)).astype(BF)
+    lf = lax.dot_general(
+        jnp.concatenate([whigh, wlow], axis=0), tokv[...], NT, preferred_element_type=F32
+    )
+    lf = lf[0:heads_all] + lf[heads_all : 2 * heads_all]
+    inv_lane = dot_hi(jnp.full((8, lanes), 1.0 / lanes, F32), invv[...], NT)[0:1]
     bcol = jnp.zeros((heads_all, rows), F32)
     for h in range(heads_all):
         bcol = jnp.where(iota((heads_all, rows), 0) == h, bias[h], bcol)
-    z = lf + bcol
+    z = lf * inv_lane + bcol
     lf = jnp.minimum(z, 0.0) - jnp.log1p(jnp.exp(-jnp.abs(z)))
     path_t = dot_hi(lf, a, NT)
     rep = hot(iota((r64, heads_all), 1) == mt * heads + iota((r64, heads_all), 0) % heads)
@@ -455,32 +530,35 @@
     ptile[...] = pt
     ptm = jnp.where((iota((r64, 128), 1) // prop) % heads == iota((r64, 128), 0) % heads, pt, 0.0)
     tpath[...] = dot_hi(take, ptm)
-
-    def reduce_part(ph):
-        total = part[ph, rrow(me)].astype(F32)
-        for d in range(1, n):
-            rs_copy(ph, d).wait_recv()
-            total = total + rs_recv[ph, d].astype(F32)
-        qkv[ph, rrow(me)] = total.astype(BF)
-        each(n, lambda d: ag_copy(ph, d).start())
-
-    for ph in range(3):
-        reduce_part(ph)
-
     in_kc.wait()
     in_vc.wait()
+
+    own = part_q[rrow(me)].astype(F32)
+    for m in range(1, n):
+        q_rs(m).wait_recv()
+        own = own + q_recv[m].astype(F32)
+    q_full[rrow(me)] = own.astype(BF)
+    each_far(n, lambda m: q_ag(m).start())
+
+    for m in zmasks[::-1]:
+        kv_yrs(m).wait_recv()
+        kv_zs[m // 2] = (
+            part_kv[rrow(flip(me, m))].astype(F32) + kv_y[m // 2].astype(F32)
+        ).astype(BF)
+        kv_zrs(m).start()
+
     same_head = iota((hp, cols), 0) // prop == iota((hp, cols), 1) % heads
     diag_l = iota((L, L), 0) == iota((L, L), 1)
 
-    def heads_of(ph, s):
-        block = qkv[ph, pl.ds(pl.multiple_of(s * prop, prop), prop), :]
+    def heads_of(ref, s, first):
+        block = ref[pl.ds(pl.multiple_of(s * prop, prop), prop), first : first + hw]
         return jnp.concatenate([block[:, h * hd : (h + 1) * hd] for h in range(heads)], axis=0)
 
     def block_part(src):
         maxes, totals, values = [], [], []
         for j in range(sp):
             s = src * sp + j
-            q = heads_of(0, s)
+            q = heads_of(q_full, s, 0)
             sc = lax.dot_general(q, kcv[s], NT, preferred_element_type=F32) * scale
             sc = jnp.where(same_head, sc + brow[pl.ds(s, 1), :], floor_value)
             m = jnp.max(sc, axis=1, keepdims=True)
@@ -494,29 +572,36 @@
         t = jnp.concatenate(totals, axis=0)
         m_lane = jnp.sum(jnp.where(diag_l, m, 0.0), axis=0, keepdims=True)
         t_lane = jnp.sum(jnp.where(diag_l, t, 0.0), axis=0, keepdims=True)
-        stats = jnp.where(iota((8, L), 0) == 0, m_lane, t_lane)
+        stats = jnp.where(iota((2, L), 0) == 0, m_lane, t_lane)
         return stats, jnp.concatenate(values, axis=0)
 
-    def remote_block(d):
-        ag_wait(0, d)
-        stats, values = block_part(down(d))
-        st_send[d] = stats
-        val_send[d] = values
-        stat_copy(d).start()
-        val_copy(d).start()
-
-    each(n, remote_block)
+    def remote_block(m):
+        q_ag(m).wait_recv()
+        stats, values = block_part(flip(me, m))
+        st_send[m] = stats
+        val_send[m] = values
+        stat_copy(m).start()
+        val_copy(m).start()
+
     stats, values = block_part(me)
     st_recv[0] = stats
     val_recv[0] = values
+    each(n, remote_block)
+
+    kv_yrs(0).wait_recv()
+    own = part_kv[rrow(me)].astype(F32) + kv_y[0].astype(F32)
+    for m in zmasks:
+        kv_zrs(m).wait_recv()
+        own = own + kv_zr[m // 2].astype(F32)
+    kv_full[rrow(me)] = own.astype(BF)
 
     fold_h = iota((rows, hp), 0)
     tmax, ttot, tval = [], [], []
     for j in range(sp):
         s = me * sp + j
-        q = heads_of(0, s)
-        k = heads_of(1, s)
-        v = heads_of(2, s)
+        q = heads_of(q_full, s, 0)
+        k = heads_of(kv_full, s, 0)
+        v = heads_of(kv_full, s, hw)
         arows = anc[pl.ds(pl.multiple_of(s * prop, prop), prop), :]
         sel = hot(fold_h == s * prop + iota((rows, hp), 1) % prop).astype(BF)
         am = jnp.dot(arows.astype(BF), sel, preferred_element_type=F32)
@@ -534,142 +619,245 @@
     tree_val = jnp.concatenate(tval, axis=0)
 
     last_lane = cand_send[...]
-    for d in range(1, n):
-        cand_copy(d).wait_recv()
-        last_lane = jnp.maximum(last_lane, cand_recv[d])
-    last_col = jnp.sum(jnp.where(diag, last_lane[0:1], 0.0), axis=1, keepdims=True)
+    for m in range(1, n):
+        cand_copy(m).wait_recv()
+        last_lane = jnp.maximum(last_lane, cand_recv[m])
+    last_col = jnp.sum(jnp.where(diag, last_lane, 0.0), axis=1, keepdims=True)
     own_rows = iota((L, 128), 0)
     own_pick = iota((L, 128), 1) == (me * sp + own_rows // hp) * heads + (own_rows % hp) // prop
-    last_own = jnp.sum(jnp.where(own_pick, last_lane[0:1], 0.0), axis=1, keepdims=True)
+    last_own = jnp.sum(jnp.where(own_pick, last_lane, 0.0), axis=1, keepdims=True)
 
     shifted_path = ptile[...]
     for b in range((span - 1).bit_length()):
         moved = pltpu.roll(shifted_path, 1 << b, 1)
         shifted_path = jnp.where((rel64 >> b) & 1 == 1, moved, shifted_path)
     off = lane - rel64
-    cum_out[...] = jnp.where((off >= 0) & (off < prop), last_col + shifted_path, cum[...])
-
-    for d in range(1, n):
-        stat_copy(d).wait_recv()
-    top = st_recv[0]
-    for d in range(1, n):
-        top = jnp.maximum(top, st_recv[d])
-    top = top[0:1]
+    cum_out[...] = jnp.where((off >= 0) & (off < prop), last_col + shifted_path, c64)
+
+    for m in range(1, n):
+        stat_copy(m).wait_recv()
+    top = st_recv[0, 0:1]
+    for m in range(1, n):
+        top = jnp.maximum(top, st_recv[m, 0:1])
 
     def col(x):
         return jnp.sum(jnp.where(diag_l, x, 0.0), axis=1, keepdims=True)
 
     cache_tot = jnp.zeros((1, L), F32)
     scales = []
-    for d in range(n):
-        sd = jnp.exp(st_recv[d, 0:1] - top)
+    for m in range(n):
+        sd = jnp.exp(st_recv[m, 0:1] - top)
         scales.append(col(sd))
-        cache_tot = cache_tot + st_recv[d, 1:2] * sd
+        cache_tot = cache_tot + st_recv[m, 1:2] * sd
     shifted = col(top) + last_own
     both = jnp.maximum(shifted, tree_max)
     cscale = jnp.exp(shifted - both)
     tscale = jnp.exp(tree_max - both)
     denom = col(cache_tot) * cscale + tree_tot * tscale
-    vals = jnp.zeros((L, hd), F32)
-    for d in range(n):
-        if d > 0:
-            val_copy(d).wait_recv()
-        vals = vals + val_recv[d].astype(F32) * scales[d]
+    vals = val_recv[0].astype(F32) * scales[0]
+    for m in range(1, n):
+        val_copy(m).wait_recv()
+        vals = vals + val_recv[m].astype(F32) * scales[m]
     attended = ((vals * cscale + tree_val * tscale) / denom).astype(BF)
     for j in range(sp):
         for h in range(heads):
             att[pl.ds(pl.multiple_of(me * R + j * prop, prop), prop), h * hd : (h + 1) * hd] = (
                 attended[j * hp + h * prop : j * hp + (h + 1) * prop]
             )
-    each(n, lambda d: att_copy(d).start())
-    each(n, lambda d: ag_wait(1, d))
-    each(n, lambda d: ag_wait(2, d))
-    out_k = pltpu.make_async_copy(qkv.at[1], k_out, loc.at[7])
-    out_v = pltpu.make_async_copy(qkv.at[2], v_out, loc.at[8])
-    out_k.start()
-    out_v.start()
+    each_far(n, lambda m: att_copy(m).start())
+
+    upper = me >= half
+
+    @pl.when(upper)
+    def _():
+        for m in [z for z in zmasks if z < half]:
+            kv_zag(m).start()
+        kv_yag(0).start()
+
+    @pl.when(jnp.logical_not(upper))
+    def _():
+        for m in [z for z in zmasks if z >= half]:
+            kv_zag(m).start()
+
     in_wo.wait()
-    each(n, att_wait)
+    each(n, lambda m: to_kv(6, m, m, att.at[rrow(me)], att.at[rrow(flip(me, m))]).wait_recv())
     full = jnp.dot(att[...], wov[...], preferred_element_type=F32).astype(BF)
     oc = o_send.shape[2]
     for t in range(nt):
         o_send[t] = full[:, t * oc : (t + 1) * oc]
 
     def o_copy(d):
-        return to_tp(0, d, o_send.at[lax.rem(mt + d, nt)], o_recv.at[d])
-
-    def sq2_copy(d):
-        return to_tp(1, d, sq2_send, sq2_recv.at[d])
-
-    each(nt, lambda d: o_copy(d).start())
+        return pltpu.make_async_remote_copy(
+            src_ref=o_send.at[flip(mt, d)],
+            dst_ref=o_recv.at[d],
+            send_sem=tssem.at[d],
+            recv_sem=trsem.at[d],
+            device_id={"tp": flip(mt, d)},
+            device_id_type=MESH,
+        )
+
+    each_far(nt, lambda d: o_copy(d).start())
+
+    @pl.when(upper)
+    def _():
+        for m in zmasks:
+            to_kv(7, m, m, kv_full.at[rrow(me)], kv_full.at[rrow(flip(me, m))]).wait_recv()
+            kv_yag(m).start()
+
     mixed = o_send[mt].astype(F32)
     for d in range(1, nt):
         o_copy(d).wait_recv()
         mixed = mixed + o_recv[d].astype(F32)
-    sq_send[...] = dot_hi(jnp.ones((8, oc), F32), mixed * mixed, NT)
-    each(n, lambda d: sq_copy(d).start())
-    sq = sq_send[...]
-    for d in range(1, n):
-        sq_copy(d).wait_recv()
-        sq = sq + sq_recv[d]
-    sq2_send[...] = sq
-    each(nt, lambda d: sq2_copy(d).start())
-    for d in range(1, nt):
-        sq2_copy(d).wait_recv()
-        sq = sq + sq2_recv[d]
-    ssum = dot_hi(sq, jnp.full((8, oc), 0.125, F32), (((0,), (0,)), ((), ())))
+    sq = dot_hi(jnp.ones((8, oc), F32), mixed * mixed, NT)[0:1]
+    sq_send[...] = sq
+
+    def sq_copy(e):
+        return pltpu.make_async_remote_copy(
+            src_ref=sq_send,
+            dst_ref=sq_recv.at[e],
+            send_sem=qssem.at[e],
+            recv_sem=qrsem.at[e],
+            device_id={"kv": flip(me, e // nt), "tp": flip(mt, e % nt)},
+            device_id_type=MESH,
+        )
+
+    each_far(everyone, lambda e: sq_copy(e).start())
+
+    order = hot(
+        iota((hp, hp), 1) == iota((hp, hp), 0) % heads * prop + iota((hp, hp), 0) // heads
+    ).astype(BF)
+
+    unroll = 4
+
+    @pl.when(upper)
+    def _():
+        for m in [0] + zmasks:
+            to_kv(
+                7, m + 1, 1, kv_full.at[rrow(me)], kv_full.at[rrow(flip(me, m + 1))]
+            ).wait_recv()
+
+        def some(i, c):
+            fresh = [
+                heads_of(kv_full, i * unroll + j, first) for j in range(unroll) for first in (0, hw)
+            ]
+            placed = jnp.dot(
+                order, jnp.concatenate(fresh, axis=1), preferred_element_type=F32
+            ).astype(BF)
+            for j in range(unroll):
+                at = 2 * j * hd
+                knew_out[i * unroll + j] = placed[:, at : at + hd]
+                vnew_out[i * unroll + j] = placed[:, at + hd : at + 2 * hd]
+            return c
+
+        lax.fori_loop(0, num_seqs // unroll, some, 0)
+
+    for e in range(1, everyone):
+        sq_copy(e).wait_recv()
+        sq = sq + sq_recv[e]
+    ssum = dot_hi(
+        jnp.broadcast_to(sq, (8, rows)), jnp.full((8, oc), 0.125, F32), (((0,), (0,)), ((), ()))
+    )
+    in_gpost.wait()
     mixed_out[...] = (mixed * lax.rsqrt(ssum / width + epsilon) * gpost[...]).astype(BF)
 
-    def drain(d):
-        for ph in range(3):
-            rs_copy(ph, d).wait_send()
-            ag_copy(ph, d).wait_send()
-        stat_copy(d).wait_send()
-        val_copy(d).wait_send()
-        cand_copy(d).wait_send()
-        att_copy(d).wait_send()
-        sq_copy(d).wait_send()
+    def drain(m):
+        q_rs(m).wait_send()
+        q_ag(m).wait_send()
+        cand_copy(m).wait_send()
+        stat_copy(m).wait_send()
+        val_copy(m).wait_send()
+        att_copy(m).wait_send()
 
     each(n, drain)
-
-    def drain_t(d):
-        o_copy(d).wait_send()
-        sq2_copy(d).wait_send()
-
-    each(nt, drain_t)
-    out_k.wait()
-    out_v.wait()
-
-
-def write_kernel(num_seqs, prop, heads, hd, span, kc, vc, kn, vn, lens, accs, k_out, v_out, buf, sin, sout):
-    base = lax.axis_index("kv") * span
-    hp = heads * prop
-    cols = heads * span
-    win = hp + 16
-    srcs, dsts, news = (kc, vc), (k_out, v_out), (kn, vn)
-    for s in range(num_seqs):
-        for i in range(2):
-            pltpu.make_async_copy(srcs[i].at[s], buf.at[i, s], sin.at[i, s]).start()
-    m = iota((win, hp), 1)
-    diff = iota((win, hp), 0) - (m % prop * heads + m // prop)
-    edge = iota((win, hd), 0)
-    for s in range(num_seqs):
-        first = (lens[s] + accs[s] - base) * heads
-        start = pl.multiple_of(jnp.clip(first // 16 * 16, 0, cols - win), 16)
-        sel = hot(diff == first - start).astype(BF)
-        here = edge - (first - start)
-        inside = (here >= 0) & (here < hp)
-        for i in range(2):
-            new = news[i][s * prop : (s + 1) * prop, :]
-            new = jnp.concatenate([new[:, h * hd : (h + 1) * hd] for h in range(heads)], axis=0)
-            placed = jnp.dot(sel, new, preferred_element_type=F32)
-            pltpu.make_async_copy(srcs[i].at[s], buf.at[i, s], sin.at[i, s]).wait()
-            old = buf[i, s, pl.ds(start, win), :].astype(F32)
-            buf[i, s, pl.ds(start, win), :] = jnp.where(inside, placed, old).astype(BF)
-            pltpu.make_async_copy(buf.at[i, s], dsts[i].at[s], sout.at[i, s]).start()
-    for s in range(num_seqs):
-        for i in range(2):
-            pltpu.make_async_copy(buf.at[i, s], dsts[i].at[s], sout.at[i, s]).wait()
+    for m in [0] + zmasks:
+        kv_yrs(m).wait_send()
+    for m in zmasks:
+        kv_zrs(m).wait_send()
+
+    @pl.when(upper)
+    def _():
+        for m in [z for z in zmasks if z < half]:
+            kv_zag(m).wait_send()
+        for m in [0] + zmasks:
+            kv_yag(m).wait_send()
+
+    @pl.when(jnp.logical_not(upper))
+    def _():
+        for m in [z for z in zmasks if z >= half]:
+            kv_zag(m).wait_send()
+
+    each(nt, lambda d: o_copy(d).wait_send())
+    each(everyone, lambda e: sq_copy(e).wait_send())
+
+
+def patch_kernel(
+    n, prop, kc, vc, knew, vnew, mixed, cum, lens, accs, k_out, v_out, mixed_out, cum_out, sem, bsem, wsem
+):
+    me = lax.axis_index("kv")
+    num_seqs, span = k_out.shape[:2]
+    out_m = pltpu.make_async_copy(mixed, mixed_out, sem.at[0])
+    out_c = pltpu.make_async_copy(cum, cum_out, sem.at[1])
+    bulk = [
+        [
+            pltpu.make_async_copy(src.at[s], dst.at[s], bsem.at[i, s])
+            for i, (src, dst) in enumerate(((kc, k_out), (vc, v_out)))
+        ]
+        for s in range(num_seqs)
+    ]
+    for row in bulk:
+        for c in row:
+            c.start()
+    out_m.start()
+    out_c.start()
+
+    def moves(act, before=None):
+        for s in range(num_seqs):
+            if before is not None:
+                before(s)
+            at = lens[s] + accs[s] - me * span
+            pairs = ((knew, k_out), (vnew, v_out))
+
+            @pl.when((at >= 0) & (at <= span - prop))
+            def _():
+                for i, (src, dst) in enumerate(pairs):
+                    act(
+                        pltpu.make_async_copy(
+                            src.at[s], dst.at[s, pl.ds(at, prop)], wsem.at[i, s]
+                        )
+                    )
+
+            @pl.when(((at > -prop) & (at < 0)) | ((at > span - prop) & (at < span)))
+            def _():
+                def one(j, c):
+                    @pl.when((at + j >= 0) & (at + j < span))
+                    def _():
+                        for i, (src, dst) in enumerate(pairs):
+                            act(
+                                pltpu.make_async_copy(
+                                    src.at[s, j], dst.at[s, at + j], wsem.at[i, s]
+                                )
+                            )
+
+                    return c
+
+                lax.fori_loop(0, prop, one, 0)
+
+    def settle(s):
+        for c in bulk[s]:
+            c.wait()
+
+    @pl.when(me >= n // 2)
+    def _():
+        moves(lambda c: c.start(), settle)
+        moves(lambda c: c.wait())
+
+    @pl.when(me < n // 2)
+    def _():
+        for s in range(num_seqs):
+            settle(s)
+
+    out_m.wait()
+    out_c.wait()
 
 
 def fast_device(
@@ -700,56 +888,58 @@
     R = sp * prop
     L = sp * heads * prop
     oc = gain_post.shape[0]
+    half = n // 2
+    everyone = n * nt
     kc = key_cache.reshape(num_seqs, cols, hd)
     vc = value_cache.reshape(num_seqs, cols, hd)
     cum = jnp.swapaxes(cum_cache, 1, 2).reshape(num_seqs * heads, span)
-    anyspec = pl.BlockSpec(memory_space=pl.ANY)
+    hbm = pl.BlockSpec(memory_space=pltpu.HBM)
     vmem = pl.BlockSpec(memory_space=pltpu.VMEM)
     smem = pl.BlockSpec(memory_space=pltpu.SMEM)
     V = pltpu.VMEM
+    S = pltpu.SMEM
     D = pltpu.SemaphoreType.DMA
-    mixed, k_new, v_new, cum_new = pl.pallas_call(
+    mixed, cum_new, knew, vnew = pl.pallas_call(
         functools.partial(layer_kernel, n, nt, num_seqs, prop, heads, hd, span),
         out_shape=(
-            jax.ShapeDtypeStruct((rows, oc), BF),
-            jax.ShapeDtypeStruct((rows, hw), BF),
-            jax.ShapeDtypeStruct((rows, hw), BF),
-            jax.ShapeDtypeStruct(cum.shape, F32),
+            V((rows, oc), BF),
+            V(cum.shape, F32),
+            V((num_seqs, heads * prop, hd), BF),
+            V((num_seqs, heads * prop, hd), BF),
         ),
-        in_specs=[
-            anyspec,
-            vmem,
-            anyspec,
-            anyspec,
-            anyspec,
-            vmem,
-            smem,
-            anyspec,
-            vmem,
-            anyspec,
-            anyspec,
-            vmem,
-            smem,
-            smem,
-            vmem,
-        ],
-        out_specs=(vmem, anyspec, anyspec, vmem),
+        in_specs=[hbm] * 15,
+        out_specs=(vmem, vmem, vmem, vmem),
         scratch_shapes=[
             V((rows, width), BF),
-            V((rows, width), BF),
+            V((1, width), F32),
             V((3,) + w_query.shape, BF),
+            V(w_forget.shape[::-1], BF),
+            S(b_forget.shape, F32),
             V(w_out.shape, BF),
+            V((1, oc), F32),
             V(kc.shape, BF),
             V(vc.shape, BF),
-            V((3, rows, hw), BF),
-            V((3, n, R, hw), BF),
-            V((3, rows, hw), BF),
-            V((n, 8, L), F32),
+            V(cum.shape, F32),
+            S(lengths.shape, jnp.int32),
+            S(accepted.shape, jnp.int32),
+            V(parent.shape, jnp.int32),
+            V((rows, 128), F32),
+            V((rows, 128), F32),
+            V((rows, w_query.shape[0]), BF),
+            V((rows, hw), BF),
+            V((n, R, hw), BF),
+            V((rows, hw), BF),
+            V((rows, 2 * hw), BF),
+            V((half, R, 2 * hw), BF),
+            V((half, R, 2 * hw), BF),
+            V((half, R, 2 * hw), BF),
+            V((rows, 2 * hw), BF),
+            V((n, 2, L), F32),
             V((n, L, hd), BF),
-            V((n, 8, L), F32),
+            V((n, 2, L), F32),
             V((n, L, hd), BF),
-            V((8, 128), F32),
-            V((n, 8, 128), F32),
+            V((1, 128), F32),
+            V((n, 1, 128), F32),
             V((num_seqs, cols), F32),
             V((rows, rows), F32),
             V((num_seqs, 128), F32),
@@ -757,53 +947,66 @@
             V((rows, hw), BF),
             V((nt, rows, oc), BF),
             V((nt, rows, oc), BF),
-            V((8, rows), F32),
-            V((n, 8, rows), F32),
-            V((8, rows), F32),
-            V((nt, 8, rows), F32),
-            D((9,)),
-            D((11, n)),
-            D((11, n)),
-            D((2, nt)),
-            D((2, nt)),
+            V((1, rows), F32),
+            V((everyone, 1, rows), F32),
+            D((18,)),
+            D((8, n)),
+            D((8, n)),
+            D((nt,)),
+            D((nt,)),
+            D((everyone,)),
+            D((everyone,)),
         ],
         compiler_params=pltpu.CompilerParams(
             collective_id=0, has_side_effects=True, vmem_limit_bytes=50 * 1024 * 1024
         ),
         name="layer",
     )(
-        tokens.reshape(rows, width),
-        gain_pre.reshape(1, width),
-        w_query,
-        w_key,
-        w_value,
-        w_forget.T,
-        b_forget,
-        w_out,
-        gain_post.reshape(1, oc),
-        kc,
-        vc,
-        cum,
+        *[
+            pltpu.with_memory_space_constraint(operand, pltpu.HBM)
+            for operand in (
+                tokens.reshape(rows, width),
+                gain_pre.reshape(1, width),
+                w_query,
+                w_key,
+                w_value,
+                w_forget.T,
+                b_forget,
+                w_out,
+                gain_post.reshape(1, oc),
+                kc,
+                vc,
+                cum,
+                lengths,
+                accepted,
+                parent,
+            )
+        ]
+    )
+    fresh = (num_seqs, prop, heads, hd)
+    key_out, value_out, mixed, cum_new = pl.pallas_call(
+        functools.partial(patch_kernel, n, prop),
+        out_shape=(
+            pltpu.HBM(key_cache.shape, BF),
+            pltpu.HBM(value_cache.shape, BF),
+            pltpu.HBM(mixed.shape, BF),
+            pltpu.HBM(cum.shape, F32),
+        ),
+        in_specs=[vmem, vmem, vmem, vmem, vmem, vmem, smem, smem],
+        out_specs=(hbm, hbm, hbm, hbm),
+        scratch_shapes=[D((2,)), D((2, num_seqs)), D((2, num_seqs))],
+        compiler_params=pltpu.CompilerParams(
+            has_side_effects=True, vmem_limit_bytes=4 * 1024 * 1024
+        ),
+        name="patch",
+    )(
+        *[
+            pltpu.with_memory_space_constraint(operand, V)
+            for operand in (key_cache, value_cache, knew.reshape(fresh), vnew.reshape(fresh), mixed, cum_new)
+        ],
         lengths,
         accepted,
-        parent,
-    )
-    key_out, value_out = pl.pallas_call(
-        functools.partial(write_kernel, num_seqs, prop, heads, hd, span),
-        out_shape=(
-            jax.ShapeDtypeStruct(kc.shape, BF),
-            jax.ShapeDtypeStruct(vc.shape, BF),
-        ),
-        in_specs=[anyspec, anyspec, vmem, vmem, smem, smem],
-        out_specs=(anyspec, anyspec),
-        scratch_shapes=[
-            V((2,) + kc.shape, BF),
-            D((2, num_seqs)),
-            D((2, num_seqs)),
-        ],
-        compiler_params=pltpu.CompilerParams(vmem_limit_bytes=16 * 1024 * 1024),
-        name="cache_write",
-    )(kc, vc, k_new, v_new, lengths, accepted)
+    )
     cum_out = jnp.swapaxes(cum_new.reshape(num_seqs, heads, span), 1, 2)
     return (
         mixed.reshape(num_seqs, prop, oc),
@@ -822,6 +1025,10 @@
         span, heads = key_cache.shape[1:3]
         fits = (
             num_seqs % n == 0
+            and n >= 4
+            and n & (n - 1) == 0
+            and nt & (nt - 1) == 0
+            and num_seqs % 4 == 0
             and (num_seqs // n) * heads * prop == 128
             and span == 128
             and num_seqs * heads <= 128

time: 98.3 us -> 60.7 us (0.62)
  Pallas kernels: 86 us -> 59.8 us
  local copies, waits for them, and re-layouts: 11.1 us -> 0.02 us
    pallas_call x1, Pallas kernels: 74.2 us -> 56.7 us  [fast_device(): pl.pallas_call(functools.partial(layer_kernel, n, nt, num_seqs, prop, hea...]
    unnamed x30 -> x8, local copies, waits for them, and re-layouts: 11.1 us -> 0.02 us
    pallas_call x1, Pallas kernels: 11.8 us -> 3.14 us  [fast_device(): pl.pallas_call(functools.partial(patch_kernel, n, prop), out_shape=(pltpu...]
where the time goes in v1:
time: 60.7 us; the launch traced here: 60.5 us
  Pallas kernels  59.8 us (99%)
  between operations  0.71 us (1%)
    pallas_call x1, Pallas kernels, fast_device(): pl.pallas_call(functools.partial(layer_kernel, n, nt, num_seqs, prop, hea...  56.7 us
    pallas_call x1, Pallas kernels, fast_device(): pl.pallas_call(functools.partial(patch_kernel, n, prop), out_shape=(pltpu...  3.14 us

profile of v1, /device:TPU:0, one launch (start us, length us, event | category | flops | bytes accessed | tf_op | source)
XLA Modules:
  0.0 60.5 jit_solution(4276924978540273913)
XLA Ops:
  0.6 0.0 copy-start
  0.6 0.0 copy-start.1
  0.7 0.0 copy-start.2
  0.7 0.0 copy-start.3
  0.7 56.7 %layer.1 = (bf16[256,128]{1,0:T(8,128)(2,1)S(1)}, f32[64,128]{1,0:T(8,128)S(1)}, bf16[16,64,128]{2,1,0:T(8,128)(2,1)S(1)}, bf16[16,64,128]{2,1,0:T(8,128)(2,1)S(1)}) custom-call(bf16[256,4096]{1,0:T(8,128)(2,1)} %bitcast.19, f32[1,4096]{1,0:T(1,128)} %bitcast.22, bf16[512,512]{1,0:T(8,128)(2,1)} %wq_h.1, bf16[512,512]{1,0:T(8,128)(2,1)} %wk_h.1, ...), custom_call_target="tpu_custom_call" | custom-call | tf_op jit(solution)/shard_map/layer/pallas_call | solution.py:902
  57.4 0.0 copy-done
  57.4 0.0 copy-done.1
  57.4 0.0 copy-done.2
  57.4 0.0 copy-done.3
  57.4 3.1 %patch.1 = (bf16[16,128,4,128]{3,2,1,0:T(4,128)(2,1)}, bf16[16,128,4,128]{3,2,1,0:T(4,128)(2,1)}, bf16[256,128]{1,0:T(8,128)(2,1)}, f32[64,128]{1,0:T(8,128)}) custom-call(bf16[16,128,4,128]{3,2,1,0:T(4,128)(2,1)S(1)} %copy-done, bf16[16,128,4,128]{3,2,1,0:T(4,128)(2,1)S(1)} %copy-done.1, bf16[16,16,4,128]{3,2,1,0:T(4,128)(2,1)S(1)} %bitcast.17, ...), custom_call_target="tpu_custom_call" | custom-call | tf_op jit(solution)/shard_map/patch/pallas_call | solution.py:987
Async XLA Ops:
  0.6 56.7 %copy-start = (bf16[16,128,4,128]{3,2,1,0:T(4,128)(2,1)S(1)}, bf16[16,128,4,128]{3,2,1,0:T(4,128)(2,1)}, u32[]{:S(2)}) copy-start(bf16[16,128,4,128]{3,2,1,0:T(4,128)(2,1)} %kc.1) | copy-start | bytes 6291460
  0.6 56.7 %copy-start.1 = (bf16[16,128,4,128]{3,2,1,0:T(4,128)(2,1)S(1)}, bf16[16,128,4,128]{3,2,1,0:T(4,128)(2,1)}, u32[]{:S(2)}) copy-start(bf16[16,128,4,128]{3,2,1,0:T(4,128)(2,1)} %vc.1) | copy-start | bytes 6291460
  0.7 56.7 %copy-start.2 = (s32[16]{0:T(128)S(1)}, s32[16]{0:T(128)}, u32[]{:S(2)}) copy-start(s32[16]{0:T(128)} %lens.1) | copy-start | bytes 196
  0.7 56.7 %copy-start.3 = (s32[16]{0:T(128)S(1)}, s32[16]{0:T(128)}, u32[]{:S(2)}) copy-start(s32[16]{0:T(128)} %accs.1) | copy-start | bytes 196

commit v2 on v1

--- a/solution.py
+++ b/solution.py
@@ -215,13 +215,14 @@
 NT = (((1,), (1,)), ((), ()))
 
 
-def flip(value, mask):
-    total = 0
+def flips(value, count):
     bit = 1
-    while bit < 64:
-        total = total + ((value // bit + mask // bit) % 2) * bit
+    out = [value]
+    while bit < count:
+        step = bit * (1 - 2 * lax.rem(lax.div(value, bit), 2))
+        out = out + [other + step for other in out]
         bit *= 2
-    return total
+    return out
 
 
 def layer_kernel(
@@ -316,14 +317,8 @@
 
     barrier = pltpu.get_barrier_semaphore()
 
-    def greet(e, c):
-        pl.semaphore_signal(
-            barrier,
-            inc=1,
-            device_id={"kv": flip(me, e // nt), "tp": flip(mt, e % nt)},
-            device_id_type=MESH,
-        )
-        return c
+    kvs = flips(me, n)
+    tps = flips(mt, nt)
 
     chunks = 4
     crow = rows // chunks
@@ -372,7 +367,13 @@
         c.start()
     for c in copies:
         c.start()
-    lax.fori_loop(1, everyone, greet, 0)
+    for e in range(1, everyone):
+        pl.semaphore_signal(
+            barrier,
+            inc=1,
+            device_id={"kv": kvs[e // nt], "tp": tps[e % nt]},
+            device_id_type=MESH,
+        )
 
     def to_kv(ph, slot, mask, src, dst):
         return pltpu.make_async_remote_copy(
@@ -380,7 +381,7 @@
             dst_ref=dst,
             send_sem=ssem.at[ph, slot],
             recv_sem=rsem.at[ph, slot],
-            device_id={"kv": flip(me, mask)},
+            device_id={"kv": kvs[mask]},
             device_id_type=MESH,
         )
 
@@ -388,13 +389,13 @@
         return pl.ds(pl.multiple_of(i * R, R), R)
 
     def q_rs(m):
-        return to_kv(0, m, m, part_q.at[rrow(flip(me, m))], q_recv.at[m])
+        return to_kv(0, m, m, part_q.at[rrow(kvs[m])], q_recv.at[m])
 
     def q_ag(m):
         return to_kv(1, m, m, q_full.at[rrow(me)], q_full.at[rrow(me)])
 
     def kv_yrs(m):
-        return to_kv(2, m, 1, part_kv.at[rrow(flip(me, m + 1))], kv_y.at[m // 2])
+        return to_kv(2, m, 1, part_kv.at[rrow(kvs[m + 1])], kv_y.at[m // 2])
 
     def kv_zrs(m):
         return to_kv(2, m + 1, m, kv_zs.at[m // 2], kv_zr.at[m // 2])
@@ -415,17 +416,15 @@
         return to_kv(7, m, m, kv_full.at[rrow(me)], kv_full.at[rrow(me)])
 
     def kv_yag(m):
-        return to_kv(7, m + 1, 1, kv_full.at[rrow(flip(me, m))], kv_full.at[rrow(flip(me, m))])
+        return to_kv(7, m + 1, 1, kv_full.at[rrow(kvs[m])], kv_full.at[rrow(kvs[m])])
 
     def each(count, fn):
-        def body(d, c):
+        for d in range(1, count):
             fn(d)
-            return c
-
-        lax.fori_loop(1, count, body, 0)
 
     def each_far(count, fn):
-        each(count, lambda d: fn(count - d))
+        for d in range(count - 1, 0, -1):
+            fn(d)
 
     zmasks = list(range(2, n, 2))
     nb = prop
@@ -543,7 +542,7 @@
     for m in zmasks[::-1]:
         kv_yrs(m).wait_recv()
         kv_zs[m // 2] = (
-            part_kv[rrow(flip(me, m))].astype(F32) + kv_y[m // 2].astype(F32)
+            part_kv[rrow(kvs[m])].astype(F32) + kv_y[m // 2].astype(F32)
         ).astype(BF)
         kv_zrs(m).start()
 
@@ -575,18 +574,23 @@
         stats = jnp.where(iota((2, L), 0) == 0, m_lane, t_lane)
         return stats, jnp.concatenate(values, axis=0)
 
-    def remote_block(m):
-        q_ag(m).wait_recv()
-        stats, values = block_part(flip(me, m))
-        st_send[m] = stats
-        val_send[m] = values
-        stat_copy(m).start()
-        val_copy(m).start()
+    def remote_blocks(masks):
+        for m in masks:
+            q_ag(m).wait_recv()
+        parts = [block_part(kvs[m]) for m in masks]
+        for m, (stats, values) in zip(masks, parts):
+            st_send[m] = stats
+            val_send[m] = values
+        for m in masks:
+            stat_copy(m).start()
+            val_copy(m).start()
 
     stats, values = block_part(me)
     st_recv[0] = stats
     val_recv[0] = values
-    each(n, remote_block)
+    remote_blocks([1])
+    for m in zmasks:
+        remote_blocks([m, m + 1])
 
     kv_yrs(0).wait_recv()
     own = part_kv[rrow(me)].astype(F32) + kv_y[0].astype(F32)
@@ -622,17 +626,9 @@
     for m in range(1, n):
         cand_copy(m).wait_recv()
         last_lane = jnp.maximum(last_lane, cand_recv[m])
-    last_col = jnp.sum(jnp.where(diag, last_lane, 0.0), axis=1, keepdims=True)
     own_rows = iota((L, 128), 0)
     own_pick = iota((L, 128), 1) == (me * sp + own_rows // hp) * heads + (own_rows % hp) // prop
     last_own = jnp.sum(jnp.where(own_pick, last_lane, 0.0), axis=1, keepdims=True)
-
-    shifted_path = ptile[...]
-    for b in range((span - 1).bit_length()):
-        moved = pltpu.roll(shifted_path, 1 << b, 1)
-        shifted_path = jnp.where((rel64 >> b) & 1 == 1, moved, shifted_path)
-    off = lane - rel64
-    cum_out[...] = jnp.where((off >= 0) & (off < prop), last_col + shifted_path, c64)
 
     for m in range(1, n):
         stat_copy(m).wait_recv()
@@ -679,34 +675,49 @@
         for m in [z for z in zmasks if z >= half]:
             kv_zag(m).start()
 
+    last_col = jnp.sum(jnp.where(diag, last_lane, 0.0), axis=1, keepdims=True)
+    shifted_path = ptile[...]
+    for b in range((span - 1).bit_length()):
+        moved = pltpu.roll(shifted_path, 1 << b, 1)
+        shifted_path = jnp.where((rel64 >> b) & 1 == 1, moved, shifted_path)
+    off = lane - rel64
+    cum_out[...] = jnp.where((off >= 0) & (off < prop), last_col + shifted_path, c64)
+
     in_wo.wait()
-    each(n, lambda m: to_kv(6, m, m, att.at[rrow(me)], att.at[rrow(flip(me, m))]).wait_recv())
-    full = jnp.dot(att[...], wov[...], preferred_element_type=F32).astype(BF)
     oc = o_send.shape[2]
-    for t in range(nt):
-        o_send[t] = full[:, t * oc : (t + 1) * oc]
-
-    def o_copy(d):
+    near = lax.div(me, half) * (half * R)
+    grows = [
+        pl.ds(pl.multiple_of(first, half * R), half * R) for first in (near, half * R - near)
+    ]
+
+    def o_copy(g, d):
         return pltpu.make_async_remote_copy(
-            src_ref=o_send.at[flip(mt, d)],
-            dst_ref=o_recv.at[d],
-            send_sem=tssem.at[d],
-            recv_sem=trsem.at[d],
-            device_id={"tp": flip(mt, d)},
+            src_ref=o_send.at[tps[d], grows[g]],
+            dst_ref=o_recv.at[d, grows[g]],
+            send_sem=tssem.at[g, d],
+            recv_sem=trsem.at[g, d],
+            device_id={"tp": tps[d]},
             device_id_type=MESH,
         )
 
-    each_far(nt, lambda d: o_copy(d).start())
+    for g in range(2):
+        for m in range(max(1, g * half), (g + 1) * half):
+            to_kv(6, m, m, att.at[rrow(me)], att.at[rrow(kvs[m])]).wait_recv()
+        full = jnp.dot(att[grows[g]], wov[...], preferred_element_type=F32).astype(BF)
+        for t in range(nt):
+            o_send[t, grows[g]] = full[:, t * oc : (t + 1) * oc]
+        each_far(nt, lambda d: o_copy(g, d).start())
 
     @pl.when(upper)
     def _():
         for m in zmasks:
-            to_kv(7, m, m, kv_full.at[rrow(me)], kv_full.at[rrow(flip(me, m))]).wait_recv()
+            to_kv(7, m, m, kv_full.at[rrow(me)], kv_full.at[rrow(kvs[m])]).wait_recv()
             kv_yag(m).start()
 
     mixed = o_send[mt].astype(F32)
     for d in range(1, nt):
-        o_copy(d).wait_recv()
+        o_copy(0, d).wait_recv()
+        o_copy(1, d).wait_recv()
         mixed = mixed + o_recv[d].astype(F32)
     sq = dot_hi(jnp.ones((8, oc), F32), mixed * mixed, NT)[0:1]
     sq_send[...] = sq
@@ -717,7 +728,7 @@
             dst_ref=sq_recv.at[e],
             send_sem=qssem.at[e],
             recv_sem=qrsem.at[e],
-            device_id={"kv": flip(me, e // nt), "tp": flip(mt, e % nt)},
+            device_id={"kv": kvs[e // nt], "tp": tps[e % nt]},
             device_id_type=MESH,
         )
 
@@ -733,7 +744,7 @@
     def _():
         for m in [0] + zmasks:
             to_kv(
-                7, m + 1, 1, kv_full.at[rrow(me)], kv_full.at[rrow(flip(me, m + 1))]
+                7, m + 1, 1, kv_full.at[rrow(me)], kv_full.at[rrow(kvs[m + 1])]
             ).wait_recv()
 
         def some(i, c):
@@ -786,7 +797,8 @@
         for m in [z for z in zmasks if z >= half]:
             kv_zag(m).wait_send()
 
-    each(nt, lambda d: o_copy(d).wait_send())
+    for g in range(2):
+        each(nt, lambda d: o_copy(g, d).wait_send())
     each(everyone, lambda e: sq_copy(e).wait_send())
 
 
@@ -952,8 +964,8 @@
             D((18,)),
             D((8, n)),
             D((8, n)),
-            D((nt,)),
-            D((nt,)),
+            D((2, nt)),
+            D((2, nt)),
             D((everyone,)),
             D((everyone,)),
         ],

time: 60.7 us -> 58 us (0.956)
  Pallas kernels: 59.8 us -> 57.1 us
    pallas_call x1, Pallas kernels: 56.7 us -> 54 us  [fast_device(): pl.pallas_call(functools.partial(layer_kernel, n, nt, num_seqs, prop, hea...]
where the time goes in v2:
time: 58 us; the launch traced here: 57.8 us
  Pallas kernels  57.1 us (98%)
  between operations  0.71 us (1%)
    pallas_call x1, Pallas kernels, fast_device(): pl.pallas_call(functools.partial(layer_kernel, n, nt, num_seqs, prop, hea...  54 us
    pallas_call x1, Pallas kernels, fast_device(): pl.pallas_call(functools.partial(patch_kernel, n, prop), out_shape=(pltpu...  3.14 us

profile of v2, /device:TPU:0, one launch (start us, length us, event | category | flops | bytes accessed | tf_op | source)
XLA Modules:
  0.0 57.8 jit_solution(9487712927953253889)
XLA Ops:
  0.6 0.0 copy-start
  0.6 0.0 copy-start.1
  0.7 0.0 copy-start.2
  0.7 0.0 copy-start.3
  0.7 54.0 %layer.1 = (bf16[256,128]{1,0:T(8,128)(2,1)S(1)}, f32[64,128]{1,0:T(8,128)S(1)}, bf16[16,64,128]{2,1,0:T(8,128)(2,1)S(1)}, bf16[16,64,128]{2,1,0:T(8,128)(2,1)S(1)}) custom-call(bf16[256,4096]{1,0:T(8,128)(2,1)} %bitcast.19, f32[1,4096]{1,0:T(1,128)} %bitcast.22, bf16[512,512]{1,0:T(8,128)(2,1)} %wq_h.1, bf16[512,512]{1,0:T(8,128)(2,1)} %wk_h.1, ...), custom_call_target="tpu_custom_call" | custom-call | tf_op jit(solution)/shard_map/layer/pallas_call | solution.py:914
  54.7 0.0 copy-done
  54.7 0.0 copy-done.1
  54.7 0.0 copy-done.2
  54.7 0.0 copy-done.3
  54.7 3.1 %patch.1 = (bf16[16,128,4,128]{3,2,1,0:T(4,128)(2,1)}, bf16[16,128,4,128]{3,2,1,0:T(4,128)(2,1)}, bf16[256,128]{1,0:T(8,128)(2,1)}, f32[64,128]{1,0:T(8,128)}) custom-call(bf16[16,128,4,128]{3,2,1,0:T(4,128)(2,1)S(1)} %copy-done, bf16[16,128,4,128]{3,2,1,0:T(4,128)(2,1)S(1)} %copy-done.1, bf16[16,16,4,128]{3,2,1,0:T(4,128)(2,1)S(1)} %bitcast.17, ...), custom_call_target="tpu_custom_call" | custom-call | tf_op jit(solution)/shard_map/patch/pallas_call | solution.py:999
Async XLA Ops:
  0.6 54.0 %copy-start = (bf16[16,128,4,128]{3,2,1,0:T(4,128)(2,1)S(1)}, bf16[16,128,4,128]{3,2,1,0:T(4,128)(2,1)}, u32[]{:S(2)}) copy-start(bf16[16,128,4,128]{3,2,1,0:T(4,128)(2,1)} %kc.1) | copy-start | bytes 6291460
  0.6 54.0 %copy-start.1 = (bf16[16,128,4,128]{3,2,1,0:T(4,128)(2,1)S(1)}, bf16[16,128,4,128]{3,2,1,0:T(4,128)(2,1)}, u32[]{:S(2)}) copy-start(bf16[16,128,4,128]{3,2,1,0:T(4,128)(2,1)} %vc.1) | copy-start | bytes 6291460
  0.7 54.0 %copy-start.2 = (s32[16]{0:T(128)S(1)}, s32[16]{0:T(128)}, u32[]{:S(2)}) copy-start(s32[16]{0:T(128)} %lens.1) | copy-start | bytes 196
  0.7 54.0 %copy-start.3 = (s32[16]{0:T(128)S(1)}, s32[16]{0:T(128)}, u32[]{:S(2)}) copy-start(s32[16]{0:T(128)} %accs.1) | copy-start | bytes 196

commit v3 on v2

--- a/solution.py
+++ b/solution.py
@@ -269,7 +269,9 @@
     invv,
     xloc,
     part_q,
-    q_recv,
+    q_y,
+    q_zs,
+    q_zr,
     q_full,
     part_kv,
     kv_y,
@@ -388,11 +390,17 @@
     def rrow(i):
         return pl.ds(pl.multiple_of(i * R, R), R)
 
-    def q_rs(m):
-        return to_kv(0, m, m, part_q.at[rrow(kvs[m])], q_recv.at[m])
+    def q_yrs(m):
+        return to_kv(0, m, 1, part_q.at[rrow(kvs[m + 1])], q_y.at[m // 2])
+
+    def q_zrs(m):
+        return to_kv(0, m + 1, m, q_zs.at[m // 2], q_zr.at[m // 2])
+
+    def spread_to(ph, slot, mask, ref, rank):
+        return to_kv(ph, slot, mask, ref.at[rrow(rank)], ref.at[rrow(rank)])
 
     def q_ag(m):
-        return to_kv(1, m, m, q_full.at[rrow(me)], q_full.at[rrow(me)])
+        return spread_to(1, m, 1, q_full, kvs[m - 1]) if m % 2 else spread_to(1, m, m, q_full, me)
 
     def kv_yrs(m):
         return to_kv(2, m, 1, part_kv.at[rrow(kvs[m + 1])], kv_y.at[m // 2])
@@ -409,14 +417,17 @@
     def val_copy(m):
         return to_kv(5, m, m, val_send.at[m], val_recv.at[m])
 
-    def att_copy(m):
-        return to_kv(6, m, m, att.at[rrow(me)], att.at[rrow(me)])
-
-    def kv_zag(m):
-        return to_kv(7, m, m, kv_full.at[rrow(me)], kv_full.at[rrow(me)])
-
-    def kv_yag(m):
-        return to_kv(7, m + 1, 1, kv_full.at[rrow(kvs[m])], kv_full.at[rrow(kvs[m])])
+    def att_ag(m):
+        return spread_to(6, m, 1, att, kvs[m - 1]) if m % 2 else spread_to(6, m, m, att, me)
+
+    def kv_cross():
+        return spread_to(7, half, half, kv_full, me)
+
+    def kv_pass(m):
+        return spread_to(7, m, half // 2, kv_full, kvs[m - half // 2])
+
+    def kv_side(m):
+        return spread_to(7, m, 1, kv_full, kvs[m - 1])
 
     def each(count, fn):
         for d in range(1, count):
@@ -455,7 +466,8 @@
     in_wq.wait()
     part_q[...] = jnp.dot(xloc[...], wqkv[0], preferred_element_type=F32).astype(BF)
     pl.semaphore_wait(barrier, everyone - 1)
-    each_far(n, lambda m: q_rs(m).start())
+    for m in zmasks[::-1] + [0]:
+        q_yrs(m).start()
     in_wk.wait()
     in_wv.wait()
     part_kv[:, 0:hw] = jnp.dot(xloc[...], wqkv[1], preferred_element_type=F32).astype(BF)
@@ -505,6 +517,10 @@
         low = a.astype(BF)
         a = jnp.minimum(jnp.dot(low, low, preferred_element_type=F32), 1.0)
     anc[...] = a
+    for m in zmasks[::-1]:
+        q_yrs(m).wait_recv()
+        q_zs[m // 2] = (part_q[rrow(kvs[m])].astype(F32) + q_y[m // 2].astype(F32)).astype(BF)
+        q_zrs(m).start()
     in_wft.wait()
     in_bias.wait()
     wscaled = wft[...].astype(F32) * gain[...]
@@ -532,12 +548,14 @@
     in_kc.wait()
     in_vc.wait()
 
-    own = part_q[rrow(me)].astype(F32)
-    for m in range(1, n):
-        q_rs(m).wait_recv()
-        own = own + q_recv[m].astype(F32)
+    q_yrs(0).wait_recv()
+    own = part_q[rrow(me)].astype(F32) + q_y[0].astype(F32)
+    for m in zmasks:
+        q_zrs(m).wait_recv()
+        own = own + q_zr[m // 2].astype(F32)
     q_full[rrow(me)] = own.astype(BF)
-    each_far(n, lambda m: q_ag(m).start())
+    for m in [1] + zmasks[::-1]:
+        q_ag(m).start()
 
     for m in zmasks[::-1]:
         kv_yrs(m).wait_recv()
@@ -575,8 +593,6 @@
         return stats, jnp.concatenate(values, axis=0)
 
     def remote_blocks(masks):
-        for m in masks:
-            q_ag(m).wait_recv()
         parts = [block_part(kvs[m]) for m in masks]
         for m, (stats, values) in zip(masks, parts):
             st_send[m] = stats
@@ -588,9 +604,22 @@
     stats, values = block_part(me)
     st_recv[0] = stats
     val_recv[0] = values
-    remote_blocks([1])
-    for m in zmasks:
-        remote_blocks([m, m + 1])
+    def take_q(m):
+        q_ag(m).wait_recv()
+        if m % 2 == 0:
+            q_ag(m + 1).start()
+
+    take_q(2)
+    take_q(1)
+    remote_blocks([1, 2])
+    take_q(4)
+    take_q(6)
+    remote_blocks([4, 6])
+    take_q(3)
+    take_q(5)
+    remote_blocks([3, 5])
+    take_q(7)
+    remote_blocks([7])
 
     kv_yrs(0).wait_recv()
     own = part_kv[rrow(me)].astype(F32) + kv_y[0].astype(F32)
@@ -660,20 +689,19 @@
             att[pl.ds(pl.multiple_of(me * R + j * prop, prop), prop), h * hd : (h + 1) * hd] = (
                 attended[j * hp + h * prop : j * hp + (h + 1) * prop]
             )
-    each_far(n, lambda m: att_copy(m).start())
+    for m in [1] + zmasks[::-1]:
+        att_ag(m).start()
 
     upper = me >= half
 
     @pl.when(upper)
     def _():
-        for m in [z for z in zmasks if z < half]:
-            kv_zag(m).start()
-        kv_yag(0).start()
+        kv_pass(2).start()
+        kv_side(1).start()
 
     @pl.when(jnp.logical_not(upper))
     def _():
-        for m in [z for z in zmasks if z >= half]:
-            kv_zag(m).start()
+        kv_cross().start()
 
     last_col = jnp.sum(jnp.where(diag, last_lane, 0.0), axis=1, keepdims=True)
     shifted_path = ptile[...]
@@ -700,9 +728,12 @@
             device_id_type=MESH,
         )
 
+    for m in zmasks:
+        att_ag(m).wait_recv()
+        att_ag(m + 1).start()
     for g in range(2):
-        for m in range(max(1, g * half), (g + 1) * half):
-            to_kv(6, m, m, att.at[rrow(me)], att.at[rrow(kvs[m])]).wait_recv()
+        for m in range(1 + g * half, (g + 1) * half, 2):
+            att_ag(m).wait_recv()
         full = jnp.dot(att[grows[g]], wov[...], preferred_element_type=F32).astype(BF)
         for t in range(nt):
             o_send[t, grows[g]] = full[:, t * oc : (t + 1) * oc]
@@ -710,9 +741,11 @@
 
     @pl.when(upper)
     def _():
-        for m in zmasks:
-            to_kv(7, m, m, kv_full.at[rrow(me)], kv_full.at[rrow(kvs[m])]).wait_recv()
-            kv_yag(m).start()
+        kv_cross().wait_recv()
+        kv_pass(6).start()
+        kv_side(5).start()
+        kv_pass(2).wait_recv()
+        kv_side(3).start()
 
     mixed = o_send[mt].astype(F32)
     for d in range(1, nt):
@@ -742,10 +775,10 @@
 
     @pl.when(upper)
     def _():
-        for m in [0] + zmasks:
-            to_kv(
-                7, m + 1, 1, kv_full.at[rrow(me)], kv_full.at[rrow(kvs[m + 1])]
-            ).wait_recv()
+        kv_pass(6).wait_recv()
+        kv_side(7).start()
+        for m in range(1, n, 2):
+            kv_side(m).wait_recv()
 
         def some(i, c):
             fresh = [
@@ -772,30 +805,30 @@
     mixed_out[...] = (mixed * lax.rsqrt(ssum / width + epsilon) * gpost[...]).astype(BF)
 
     def drain(m):
-        q_rs(m).wait_send()
         q_ag(m).wait_send()
         cand_copy(m).wait_send()
         stat_copy(m).wait_send()
         val_copy(m).wait_send()
-        att_copy(m).wait_send()
+        att_ag(m).wait_send()
 
     each(n, drain)
     for m in [0] + zmasks:
+        q_yrs(m).wait_send()
         kv_yrs(m).wait_send()
     for m in zmasks:
+        q_zrs(m).wait_send()
         kv_zrs(m).wait_send()
 
     @pl.when(upper)
     def _():
-        for m in [z for z in zmasks if z < half]:
-            kv_zag(m).wait_send()
-        for m in [0] + zmasks:
-            kv_yag(m).wait_send()
+        for m in (2, 6):
+            kv_pass(m).wait_send()
+        for m in range(1, n, 2):
+            kv_side(m).wait_send()
 
     @pl.when(jnp.logical_not(upper))
     def _():
-        for m in [z for z in zmasks if z >= half]:
-            kv_zag(m).wait_send()
+        kv_cross().wait_send()
 
     for g in range(2):
         each(nt, lambda d: o_copy(g, d).wait_send())
@@ -939,7 +972,9 @@
             V((rows, 128), F32),
             V((rows, w_query.shape[0]), BF),
             V((rows, hw), BF),
-            V((n, R, hw), BF),
+            V((half, R, hw), BF),
+            V((half, R, hw), BF),
+            V((half, R, hw), BF),
             V((rows, hw), BF),
             V((rows, 2 * hw), BF),
             V((half, R, 2 * hw), BF),
@@ -1037,8 +1072,7 @@
         span, heads = key_cache.shape[1:3]
         fits = (
             num_seqs % n == 0
-            and n >= 4
-            and n & (n - 1) == 0
+            and n == 8
             and nt & (nt - 1) == 0
             and num_seqs % 4 == 0
             and (num_seqs // n) * heads * prop == 128

time: 58 us -> 54.1 us (0.933)
  Pallas kernels: 57.1 us -> 53.3 us
    pallas_call x1, Pallas kernels: 54 us -> 50.1 us  [fast_device(): pl.pallas_call(functools.partial(layer_kernel, n, nt, num_seqs, prop, hea...]
where the time goes in v3:
time: 54.1 us; the launch traced here: 54 us
  Pallas kernels  53.3 us (99%)
  between operations  0.71 us (1%)
    pallas_call x1, Pallas kernels, fast_device(): pl.pallas_call(functools.partial(layer_kernel, n, nt, num_seqs, prop, hea...  50.1 us
    pallas_call x1, Pallas kernels, fast_device(): pl.pallas_call(functools.partial(patch_kernel, n, prop), out_shape=(pltpu...  3.14 us

profile of v3, /device:TPU:0, one launch (start us, length us, event | category | flops | bytes accessed | tf_op | source)
XLA Modules:
  0.0 54.0 jit_solution(10632461215320262635)
XLA Ops:
  0.6 0.0 copy-start
  0.6 0.0 copy-start.1
  0.7 0.0 copy-start.2
  0.7 0.0 copy-start.3
  0.7 50.1 %layer.1 = (bf16[256,128]{1,0:T(8,128)(2,1)S(1)}, f32[64,128]{1,0:T(8,128)S(1)}, bf16[16,64,128]{2,1,0:T(8,128)(2,1)S(1)}, bf16[16,64,128]{2,1,0:T(8,128)(2,1)S(1)}) custom-call(bf16[256,4096]{1,0:T(8,128)(2,1)} %bitcast.19, f32[1,4096]{1,0:T(1,128)} %bitcast.22, bf16[512,512]{1,0:T(8,128)(2,1)} %wq_h.1, bf16[512,512]{1,0:T(8,128)(2,1)} %wk_h.1, ...), custom_call_target="tpu_custom_call" | custom-call | tf_op jit(solution)/shard_map/layer/pallas_call | solution.py:947
  50.8 0.0 copy-done
  50.8 0.0 copy-done.1
  50.8 0.0 copy-done.2
  50.8 0.0 copy-done.3
  50.8 3.1 %patch.1 = (bf16[16,128,4,128]{3,2,1,0:T(4,128)(2,1)}, bf16[16,128,4,128]{3,2,1,0:T(4,128)(2,1)}, bf16[256,128]{1,0:T(8,128)(2,1)}, f32[64,128]{1,0:T(8,128)}) custom-call(bf16[16,128,4,128]{3,2,1,0:T(4,128)(2,1)S(1)} %copy-done, bf16[16,128,4,128]{3,2,1,0:T(4,128)(2,1)S(1)} %copy-done.1, bf16[16,16,4,128]{3,2,1,0:T(4,128)(2,1)S(1)} %bitcast.17, ...), custom_call_target="tpu_custom_call" | custom-call | tf_op jit(solution)/shard_map/patch/pallas_call | solution.py:1034
Async XLA Ops:
  0.6 50.2 %copy-start = (bf16[16,128,4,128]{3,2,1,0:T(4,128)(2,1)S(1)}, bf16[16,128,4,128]{3,2,1,0:T(4,128)(2,1)}, u32[]{:S(2)}) copy-start(bf16[16,128,4,128]{3,2,1,0:T(4,128)(2,1)} %kc.1) | copy-start | bytes 6291460
  0.6 50.2 %copy-start.1 = (bf16[16,128,4,128]{3,2,1,0:T(4,128)(2,1)S(1)}, bf16[16,128,4,128]{3,2,1,0:T(4,128)(2,1)}, u32[]{:S(2)}) copy-start(bf16[16,128,4,128]{3,2,1,0:T(4,128)(2,1)} %vc.1) | copy-start | bytes 6291460
  0.7 50.2 %copy-start.2 = (s32[16]{0:T(128)S(1)}, s32[16]{0:T(128)}, u32[]{:S(2)}) copy-start(s32[16]{0:T(128)} %lens.1) | copy-start | bytes 196
  0.7 50.2 %copy-start.3 = (s32[16]{0:T(128)S(1)}, s32[16]{0:T(128)}, u32[]{:S(2)}) copy-start(s32[16]{0:T(128)} %accs.1) | copy-start | bytes 196

commit v4 on v3

--- a/solution.py
+++ b/solution.py
@@ -252,6 +252,8 @@
     cum_out,
     knew_out,
     vnew_out,
+    kcv,
+    vcv,
     tokv,
     gain,
     wqkv,
@@ -259,8 +261,6 @@
     bias,
     wov,
     gpost,
-    kcv,
-    vcv,
     cum,
     lens,
     accs,
@@ -296,10 +296,6 @@
     loc,
     ssem,
     rsem,
-    tssem,
-    trsem,
-    qssem,
-    qrsem,
 ):
     me = lax.axis_index("kv")
     mt = lax.axis_index("tp")
@@ -342,9 +338,9 @@
         (parent_h, parent),
         (cum_h, cum),
         (gpost_h, gpost),
+        (wo_h, wov),
         (kc_h, kcv),
         (vc_h, vcv),
-        (wo_h, wov),
     ]
     copies = [
         pltpu.make_async_copy(src, dst, loc.at[chunks + i]) for i, (src, dst) in enumerate(later)
@@ -361,13 +357,13 @@
         in_parent,
         in_cum,
         in_gpost,
+        in_wo,
         in_kc,
         in_vc,
-        in_wo,
     ) = copies
     for c in in_tok:
         c.start()
-    for c in copies:
+    for c in copies[:-3]:
         c.start()
     for e in range(1, everyone):
         pl.semaphore_signal(
@@ -377,57 +373,82 @@
             device_id_type=MESH,
         )
 
-    def to_kv(ph, slot, mask, src, dst):
+    def send(kind, slot, device, src, dst):
         return pltpu.make_async_remote_copy(
             src_ref=src,
             dst_ref=dst,
-            send_sem=ssem.at[ph, slot],
-            recv_sem=rsem.at[ph, slot],
-            device_id={"kv": kvs[mask]},
+            send_sem=ssem.at[kind],
+            recv_sem=rsem.at[slot],
+            device_id=device,
             device_id_type=MESH,
         )
 
+    def to_kv(kind, slot, mask, src, dst):
+        return send(kind, slot, {"kv": kvs[mask]}, src, dst)
+
     def rrow(i):
         return pl.ds(pl.multiple_of(i * R, R), R)
 
+    def spread_to(kind, slot, mask, ref, rank):
+        return to_kv(kind, slot, mask, ref.at[rrow(rank)], ref.at[rrow(rank)])
+
+    def sent(kind, ref):
+        to_kv(kind, 0, 1, ref, ref).wait_send()
+
+    def received(slot, ref):
+        to_kv(0, slot, 1, ref, ref).wait_recv()
+
+    flat = [0]
+
+    def slots(count):
+        flat[0] += count
+        return flat[0] - count
+
+    on_qy, on_qz, on_ky, on_kz = slots(half), slots(1), slots(half), slots(1)
+    on_qag, on_cand, on_stat, on_val = slots(n), slots(1), slots(1), slots(n)
+    on_att, on_kvag, on_o, on_sq = slots(n), slots(n), slots(2), slots(1)
+    last = n - 1
+
     def q_yrs(m):
-        return to_kv(0, m, 1, part_q.at[rrow(kvs[m + 1])], q_y.at[m // 2])
+        return to_kv(0, on_qy + m // 2, 1, part_q.at[rrow(kvs[m + 1])], q_y.at[m // 2])
 
     def q_zrs(m):
-        return to_kv(0, m + 1, m, q_zs.at[m // 2], q_zr.at[m // 2])
-
-    def spread_to(ph, slot, mask, ref, rank):
-        return to_kv(ph, slot, mask, ref.at[rrow(rank)], ref.at[rrow(rank)])
+        return to_kv(1, on_qz, m, q_zs.at[m // 2], q_zr.at[m // 2])
+
+    def kv_yrs(m):
+        src = part_kv.at[rrow(kvs[(m + 1) ^ last])]
+        return to_kv(2, on_ky + m // 2, 1, src, kv_y.at[m // 2])
+
+    def kv_zrs(m):
+        return to_kv(3, on_kz, m, kv_zs.at[m // 2], kv_zr.at[m // 2])
 
     def q_ag(m):
-        return spread_to(1, m, 1, q_full, kvs[m - 1]) if m % 2 else spread_to(1, m, m, q_full, me)
-
-    def kv_yrs(m):
-        return to_kv(2, m, 1, part_kv.at[rrow(kvs[m + 1])], kv_y.at[m // 2])
-
-    def kv_zrs(m):
-        return to_kv(2, m + 1, m, kv_zs.at[m // 2], kv_zr.at[m // 2])
+        if m % 2:
+            return spread_to(4, on_qag + m, 1, q_full, kvs[m - 1])
+        return spread_to(4, on_qag + m, m, q_full, me)
 
     def cand_copy(m):
-        return to_kv(3, m, m, cand_send, cand_recv.at[m])
+        return to_kv(5, on_cand, m, cand_send, cand_recv.at[m])
 
     def stat_copy(m):
-        return to_kv(4, m, m, st_send.at[m], st_recv.at[m])
+        return to_kv(6, on_stat, m, st_send.at[m], st_recv.at[m])
 
     def val_copy(m):
-        return to_kv(5, m, m, val_send.at[m], val_recv.at[m])
+        return to_kv(7, on_val + m, m, val_send.at[m], val_recv.at[m])
 
     def att_ag(m):
-        return spread_to(6, m, 1, att, kvs[m - 1]) if m % 2 else spread_to(6, m, m, att, me)
+        if m % 2:
+            return spread_to(8, on_att + m, 1, att, kvs[(m - 1) ^ last])
+        return spread_to(8, on_att + m, m, att, kvs[last])
 
     def kv_cross():
-        return spread_to(7, half, half, kv_full, me)
+        return spread_to(9, on_kvag + half, half, kv_full, kvs[last])
 
     def kv_pass(m):
-        return spread_to(7, m, half // 2, kv_full, kvs[m - half // 2])
+        return spread_to(9, on_kvag + m, half // 2, kv_full, kvs[(m - half // 2) ^ last])
 
     def kv_side(m):
-        return spread_to(7, m, 1, kv_full, kvs[m - 1])
+        return spread_to(9, on_kvag + m, 1, kv_full, kvs[(m - 1) ^ last])
 
     def each(count, fn):
         for d in range(1, count):
@@ -453,6 +474,9 @@
 
     for i in range(chunks):
         in_tok[i].wait()
+        if i == chunks - 1:
+            for c in copies[-3:]:
+                c.start()
         lax.fori_loop(i * crow // nb, (i + 1) * crow // nb, sum_rows, 0)
     total = dot_hi(ssq[...], jnp.ones((lanes, lanes), F32))
     inv = lax.rsqrt(total / width + epsilon)
@@ -550,19 +574,12 @@
 
     q_yrs(0).wait_recv()
     own = part_q[rrow(me)].astype(F32) + q_y[0].astype(F32)
+    received(on_qz, q_zr.at[pl.ds(1, half - 1)])
     for m in zmasks:
-        q_zrs(m).wait_recv()
         own = own + q_zr[m // 2].astype(F32)
     q_full[rrow(me)] = own.astype(BF)
     for m in [1] + zmasks[::-1]:
         q_ag(m).start()
-
-    for m in zmasks[::-1]:
-        kv_yrs(m).wait_recv()
-        kv_zs[m // 2] = (
-            part_kv[rrow(kvs[m])].astype(F32) + kv_y[m // 2].astype(F32)
-        ).astype(BF)
-        kv_zrs(m).start()
 
     same_head = iota((hp, cols), 0) // prop == iota((hp, cols), 1) % heads
     diag_l = iota((L, L), 0) == iota((L, L), 1)
@@ -592,18 +609,28 @@
         stats = jnp.where(iota((2, L), 0) == 0, m_lane, t_lane)
         return stats, jnp.concatenate(values, axis=0)
 
-    def remote_blocks(masks):
+    def blocks(masks):
         parts = [block_part(kvs[m]) for m in masks]
         for m, (stats, values) in zip(masks, parts):
-            st_send[m] = stats
-            val_send[m] = values
+            if m == last:
+                st_recv[0] = stats
+                val_recv[0] = values
+            else:
+                st_send[last - m] = stats
+                val_send[last - m] = values
         for m in masks:
-            stat_copy(m).start()
-            val_copy(m).start()
-
-    stats, values = block_part(me)
-    st_recv[0] = stats
-    val_recv[0] = values
+            if m != last:
+                stat_copy(last - m).start()
+                val_copy(last - m).start()
+
+    blocks([0])
+    for m in zmasks[::-1]:
+        kv_yrs(m).wait_recv()
+        kv_zs[m // 2] = (
+            part_kv[rrow(kvs[m ^ last])].astype(F32) + kv_y[m // 2].astype(F32)
+        ).astype(BF)
+        kv_zrs(m).start()
+
     def take_q(m):
         q_ag(m).wait_recv()
         if m % 2 == 0:
@@ -611,27 +638,27 @@
 
     take_q(2)
     take_q(1)
-    remote_blocks([1, 2])
+    blocks([1, 2])
     take_q(4)
     take_q(6)
-    remote_blocks([4, 6])
+    blocks([4, 6])
     take_q(3)
     take_q(5)
-    remote_blocks([3, 5])
+    blocks([3, 5])
     take_q(7)
-    remote_blocks([7])
+    blocks([7])
 
     kv_yrs(0).wait_recv()
-    own = part_kv[rrow(me)].astype(F32) + kv_y[0].astype(F32)
+    own = part_kv[rrow(kvs[last])].astype(F32) + kv_y[0].astype(F32)
+    received(on_kz, kv_zr.at[pl.ds(1, half - 1)])
     for m in zmasks:
-        kv_zrs(m).wait_recv()
         own = own + kv_zr[m // 2].astype(F32)
-    kv_full[rrow(me)] = own.astype(BF)
+    kv_full[rrow(kvs[last])] = own.astype(BF)
 
     fold_h = iota((rows, hp), 0)
     tmax, ttot, tval = [], [], []
     for j in range(sp):
-        s = me * sp + j
+        s = kvs[last] * sp + j
         q = heads_of(q_full, s, 0)
         k = heads_of(kv_full, s, 0)
         v = heads_of(kv_full, s, hw)
@@ -652,15 +679,15 @@
     tree_val = jnp.concatenate(tval, axis=0)
 
     last_lane = cand_send[...]
+    received(on_cand, cand_recv.at[pl.ds(1, n - 1)])
     for m in range(1, n):
-        cand_copy(m).wait_recv()
         last_lane = jnp.maximum(last_lane, cand_recv[m])
     own_rows = iota((L, 128), 0)
-    own_pick = iota((L, 128), 1) == (me * sp + own_rows // hp) * heads + (own_rows % hp) // prop
+    own_head = (kvs[last] * sp + own_rows // hp) * heads + (own_rows % hp) // prop
+    own_pick = iota((L, 128), 1) == own_head
     last_own = jnp.sum(jnp.where(own_pick, last_lane, 0.0), axis=1, keepdims=True)
 
-    for m in range(1, n):
-        stat_copy(m).wait_recv()
+    received(on_stat, st_recv.at[pl.ds(1, n - 1)])
     top = st_recv[0, 0:1]
     for m in range(1, n):
         top = jnp.maximum(top, st_recv[m, 0:1])
@@ -686,7 +713,7 @@
     attended = ((vals * cscale + tree_val * tscale) / denom).astype(BF)
     for j in range(sp):
         for h in range(heads):
-            att[pl.ds(pl.multiple_of(me * R + j * prop, prop), prop), h * hd : (h + 1) * hd] = (
+            att[pl.ds(pl.multiple_of(kvs[last] * R + j * prop, prop), prop), h * hd : (h + 1) * hd] = (
                 attended[j * hp + h * prop : j * hp + (h + 1) * prop]
             )
     for m in [1] + zmasks[::-1]:
@@ -713,19 +740,18 @@
 
     in_wo.wait()
     oc = o_send.shape[2]
-    near = lax.div(me, half) * (half * R)
+    near = half * R - lax.div(me, half) * (half * R)
     grows = [
         pl.ds(pl.multiple_of(first, half * R), half * R) for first in (near, half * R - near)
     ]
 
     def o_copy(g, d):
-        return pltpu.make_async_remote_copy(
-            src_ref=o_send.at[tps[d], grows[g]],
-            dst_ref=o_recv.at[d, grows[g]],
-            send_sem=tssem.at[g, d],
-            recv_sem=trsem.at[g, d],
-            device_id={"tp": tps[d]},
-            device_id_type=MESH,
+        return send(
+            10,
+            on_o + g,
+            {"tp": tps[d]},
+            o_send.at[tps[d], grows[g]],
+            o_recv.at[d, grows[g]],
         )
 
     for m in zmasks:
@@ -748,22 +774,16 @@
         kv_side(3).start()
 
     mixed = o_send[mt].astype(F32)
+    for g in range(2):
+        received(on_o + g, o_recv.at[pl.ds(1, nt - 1), grows[g]])
     for d in range(1, nt):
-        o_copy(0, d).wait_recv()
-        o_copy(1, d).wait_recv()
         mixed = mixed + o_recv[d].astype(F32)
     sq = dot_hi(jnp.ones((8, oc), F32), mixed * mixed, NT)[0:1]
     sq_send[...] = sq
 
     def sq_copy(e):
-        return pltpu.make_async_remote_copy(
-            src_ref=sq_send,
-            dst_ref=sq_recv.at[e],
-            send_sem=qssem.at[e],
-            recv_sem=qrsem.at[e],
-            device_id={"kv": kvs[e // nt], "tp": tps[e % nt]},
-            device_id_type=MESH,
-        )
+        peer = {"kv": kvs[e // nt], "tp": tps[e % nt]}
+        return send(11, on_sq, peer, sq_send, sq_recv.at[e])
 
     each_far(everyone, lambda e: sq_copy(e).start())
 
@@ -795,8 +815,8 @@
 
         lax.fori_loop(0, num_seqs // unroll, some, 0)
 
+    received(on_sq, sq_recv.at[pl.ds(1, everyone - 1)])
     for e in range(1, everyone):
-        sq_copy(e).wait_recv()
         sq = sq + sq_recv[e]
     ssum = dot_hi(
         jnp.broadcast_to(sq, (8, rows)), jnp.full((8, oc), 0.125, F32), (((0,), (0,)), ((), ()))
@@ -804,35 +824,26 @@
     in_gpost.wait()
     mixed_out[...] = (mixed * lax.rsqrt(ssum / width + epsilon) * gpost[...]).astype(BF)
 
-    def drain(m):
-        q_ag(m).wait_send()
-        cand_copy(m).wait_send()
-        stat_copy(m).wait_send()
-        val_copy(m).wait_send()
-        att_ag(m).wait_send()
-
-    each(n, drain)
-    for m in [0] + zmasks:
-        q_yrs(m).wait_send()
-        kv_yrs(m).wait_send()
-    for m in zmasks:
-        q_zrs(m).wait_send()
-        kv_zrs(m).wait_send()
+    sent(0, q_y)
+    sent(1, q_zr.at[pl.ds(1, half - 1)])
+    sent(2, kv_y)
+    sent(3, kv_zr.at[pl.ds(1, half - 1)])
+    sent(4, q_full.at[pl.ds(0, last * R)])
+    sent(5, cand_recv.at[pl.ds(1, last)])
+    sent(6, st_recv.at[pl.ds(1, last)])
+    sent(7, val_recv.at[pl.ds(1, last)])
+    sent(8, att.at[pl.ds(0, last * R)])
 
     @pl.when(upper)
     def _():
-        for m in (2, 6):
-            kv_pass(m).wait_send()
-        for m in range(1, n, 2):
-            kv_side(m).wait_send()
+        sent(9, kv_full.at[pl.ds(0, (2 + half) * R)])
 
     @pl.when(jnp.logical_not(upper))
     def _():
-        kv_cross().wait_send()
-
-    for g in range(2):
-        each(nt, lambda d: o_copy(g, d).wait_send())
-    each(everyone, lambda e: sq_copy(e).wait_send())
+        sent(9, kv_full.at[pl.ds(0, R)])
+
+    sent(10, o_recv.at[pl.ds(1, nt - 1)])
+    sent(11, sq_recv.at[pl.ds(1, everyone - 1)])
 
 
 def patch_kernel(
@@ -944,16 +955,18 @@
     V = pltpu.VMEM
     S = pltpu.SMEM
     D = pltpu.SemaphoreType.DMA
-    mixed, cum_new, knew, vnew = pl.pallas_call(
+    mixed, cum_new, knew, vnew, kv, vv = pl.pallas_call(
         functools.partial(layer_kernel, n, nt, num_seqs, prop, heads, hd, span),
         out_shape=(
             V((rows, oc), BF),
             V(cum.shape, F32),
             V((num_seqs, heads * prop, hd), BF),
             V((num_seqs, heads * prop, hd), BF),
+            V(kc.shape, BF),
+            V(vc.shape, BF),
         ),
         in_specs=[hbm] * 15,
-        out_specs=(vmem, vmem, vmem, vmem),
+        out_specs=(vmem,) * 6,
         scratch_shapes=[
             V((rows, width), BF),
             V((1, width), F32),
@@ -962,8 +975,6 @@
             S(b_forget.shape, F32),
             V(w_out.shape, BF),
             V((1, oc), F32),
-            V(kc.shape, BF),
-            V(vc.shape, BF),
             V(cum.shape, F32),
             S(lengths.shape, jnp.int32),
             S(accepted.shape, jnp.int32),
@@ -997,12 +1008,8 @@
             V((1, rows), F32),
             V((everyone, 1, rows), F32),
             D((18,)),
-            D((8, n)),
-            D((8, n)),
-            D((2, nt)),
-            D((2, nt)),
-            D((everyone,)),
-            D((everyone,)),
+            D((12,)),
+            D((2 * half + 4 * n + 7,)),
         ],
         compiler_params=pltpu.CompilerParams(
             collective_id=0, has_side_effects=True, vmem_limit_bytes=50 * 1024 * 1024
@@ -1049,7 +1056,7 @@
     )(
         *[
             pltpu.with_memory_space_constraint(operand, V)
-            for operand in (key_cache, value_cache, knew.reshape(fresh), vnew.reshape(fresh), mixed, cum_new)
+            for operand in (kv.reshape(key_cache.shape), vv.reshape(key_cache.shape), knew.reshape(fresh), vnew.reshape(fresh), mixed, cum_new)
         ],
         lengths,
         accepted,

time: 54.1 us -> 51.7 us (0.956)
  Pallas kernels: 53.3 us -> 50.8 us
    pallas_call x1, Pallas kernels: 50.1 us -> 47.7 us  [fast_device(): pl.pallas_call(functools.partial(layer_kernel, n, nt, num_seqs, prop, hea...]
where the time goes in v4:
time: 51.7 us; the launch traced here: 51.5 us
  Pallas kernels  50.8 us (98%)
  between operations  0.68 us (1%)
    pallas_call x1, Pallas kernels, fast_device(): pl.pallas_call(functools.partial(layer_kernel, n, nt, num_seqs, prop, hea...  47.7 us
    pallas_call x1, Pallas kernels, fast_device(): pl.pallas_call(functools.partial(patch_kernel, n, prop), out_shape=(pltpu...  3.14 us

profile of v4, /device:TPU:0, one launch (start us, length us, event | category | flops | bytes accessed | tf_op | source)
XLA Modules:
  0.0 51.5 jit_solution(8968364447083621053)
XLA Ops:
  0.6 0.0 copy-start
  0.6 0.0 copy-start.1
  0.7 47.7 %layer.1 = (bf16[256,128]{1,0:T(8,128)(2,1)S(1)}, f32[64,128]{1,0:T(8,128)S(1)}, bf16[16,64,128]{2,1,0:T(8,128)(2,1)S(1)}, bf16[16,64,128]{2,1,0:T(8,128)(2,1)S(...) custom-call(bf16[256,4096]{1,0:T(8,128)(2,1)} %bitcast.21, f32[1,4096]{1,0:T(1,128)} %bitcast.26, ...), custom_call_target="tpu_custom_call" | custom-call | tf_op jit(solution)/shard_map/layer/pallas_call | solution.py:958
  48.4 0.0 copy-done
  48.4 0.0 copy-done.1
  48.4 3.1 %patch.1 = (bf16[16,128,4,128]{3,2,1,0:T(4,128)(2,1)}, bf16[16,128,4,128]{3,2,1,0:T(4,128)(2,1)}, bf16[256,128]{1,0:T(8,128)(2,1)}, f32[64,128]{1,0:T(8,128)}) custom-call(bf16[16,128,4,128]{3,2,1,0:T(4,128)(2,1)S(1)} %bitcast.17, bf16[16,128,4,128]{3,2,1,0:T(4,128)(2,1)S(1)} %bitcast.18, bf16[16,16,4,128]{3,2,1,0:T(4,128)(2,1)S(1)} %bitcast.19, ...), custom_call_target="tpu_custom_call" | custom-call | tf_op jit(solution)/shard_map/patch/pallas_call | solution.py:1041
Async XLA Ops:
  0.6 47.7 %copy-start = (s32[16]{0:T(128)S(1)}, s32[16]{0:T(128)}, u32[]{:S(2)}) copy-start(s32[16]{0:T(128)} %lens.1) | copy-start | bytes 196
  0.6 47.7 %copy-start.1 = (s32[16]{0:T(128)S(1)}, s32[16]{0:T(128)}, u32[]{:S(2)}) copy-start(s32[16]{0:T(128)} %accs.1) | copy-start | bytes 196

commit v5 on v4

--- a/solution.py
+++ b/solution.py
@@ -267,6 +267,7 @@
     parent,
     ssq,
     invv,
+    xraw,
     xloc,
     part_q,
     q_y,
@@ -318,52 +319,46 @@
     kvs = flips(me, n)
     tps = flips(mt, nt)
 
-    chunks = 4
-    crow = rows // chunks
-    in_tok = [
-        pltpu.make_async_copy(
-            tok_h.at[pl.ds(i * crow, crow)], tokv.at[pl.ds(i * crow, crow)], loc.at[i]
-        )
-        for i in range(chunks)
-    ]
-    later = [
+    mine = pl.ds(pl.multiple_of(me * kdim, kdim), kdim)
+    loads = [
+        (tok_h.at[:, mine], xraw),
+        (wq_h, wqkv.at[0]),
         (gain_h, gain),
-        (wq_h, wqkv.at[0]),
         (wk_h, wqkv.at[1]),
         (wv_h, wqkv.at[2]),
+        (tok_h, tokv),
+        (lens_h, lens),
+        (accs_h, accs),
+        (cum_h, cum),
+        (parent_h, parent),
         (wft_h, wft),
         (bias_h, bias),
-        (lens_h, lens),
-        (accs_h, accs),
-        (parent_h, parent),
-        (cum_h, cum),
         (gpost_h, gpost),
-        (wo_h, wov),
         (kc_h, kcv),
         (vc_h, vcv),
+        (wo_h, wov),
     ]
-    copies = [
-        pltpu.make_async_copy(src, dst, loc.at[chunks + i]) for i, (src, dst) in enumerate(later)
-    ]
+    copies = [pltpu.make_async_copy(src, dst, loc.at[i]) for i, (src, dst) in enumerate(loads)]
     (
+        in_x,
+        in_wq,
         in_gain,
-        in_wq,
         in_wk,
         in_wv,
+        in_tok,
+        in_lens,
+        in_accs,
+        in_cum,
+        in_parent,
         in_wft,
         in_bias,
-        in_lens,
-        in_accs,
-        in_parent,
-        in_cum,
         in_gpost,
-        in_wo,
         in_kc,
         in_vc,
+        in_wo,
     ) = copies
-    for c in in_tok:
-        c.start()
-    for c in copies[:-3]:
+    urgent = 5
+    for c in copies[:urgent]:
         c.start()
     for e in range(1, everyone):
         pl.semaphore_signal(
@@ -404,7 +399,7 @@
         flat[0] += count
         return flat[0] - count
 
-    on_qy, on_qz, on_ky, on_kz = slots(half), slots(1), slots(half), slots(1)
+    on_qy, on_qz, on_ky, on_kz = slots(half), slots(1), slots(half), slots(2)
     on_qag, on_cand, on_stat, on_val = slots(n), slots(1), slots(1), slots(n)
     on_att, on_kvag, on_o, on_sq = slots(n), slots(n), slots(2), slots(1)
     last = n - 1
@@ -419,36 +414,39 @@
         src = part_kv.at[rrow(kvs[(m + 1) ^ last])]
         return to_kv(2, on_ky + m // 2, 1, src, kv_y.at[m // 2])
 
-    def kv_zrs(m):
-        return to_kv(3, on_kz, m, kv_zs.at[m // 2], kv_zr.at[m // 2])
+    def kv_near():
+        return to_kv(3, on_kz, 2, kv_zs.at[pl.ds(0, 2)], kv_zr.at[pl.ds(0, 2)])
+
+    def kv_far():
+        return to_kv(4, on_kz + 1, half, kv_zs.at[2], kv_zr.at[2])
 
     def q_ag(m):
         if m % 2:
-            return spread_to(4, on_qag + m, 1, q_full, kvs[m - 1])
-        return spread_to(4, on_qag + m, m, q_full, me)
+            return spread_to(5, on_qag + m, 1, q_full, kvs[m - 1])
+        return spread_to(5, on_qag + m, m, q_full, me)
 
     def cand_copy(m):
-        return to_kv(5, on_cand, m, cand_send, cand_recv.at[m])
+        return to_kv(6, on_cand, m, cand_send, cand_recv.at[m])
 
     def stat_copy(m):
-        return to_kv(6, on_stat, m, st_send.at[m], st_recv.at[m])
+        return to_kv(7, on_stat, m, st_send.at[m], st_recv.at[m])
 
     def val_copy(m):
-        return to_kv(7, on_val + m, m, val_send.at[m], val_recv.at[m])
+        return to_kv(8, on_val + m, m, val_send.at[m], val_recv.at[m])
 
     def att_ag(m):
         if m % 2:
-            return spread_to(8, on_att + m, 1, att, kvs[(m - 1) ^ last])
-        return spread_to(8, on_att + m, m, att, kvs[last])
+            return spread_to(9, on_att + m, 1, att, kvs[(m - 1) ^ last])
+        return spread_to(9, on_att + m, m, att, kvs[last])
 
     def kv_cross():
-        return spread_to(9, on_kvag + half, half, kv_full, kvs[last])
+        return spread_to(10, on_kvag + half, half, kv_full, kvs[last])
 
     def kv_pass(m):
-        return spread_to(9, on_kvag + m, half // 2, kv_full, kvs[(m - half // 2) ^ last])
+        return spread_to(10, on_kvag + m, half // 2, kv_full, kvs[(m - half // 2) ^ last])
 
     def kv_side(m):
-        return spread_to(9, on_kvag + m, 1, kv_full, kvs[(m - 1) ^ last])
+        return spread_to(10, on_kvag + m, 1, kv_full, kvs[(m - 1) ^ last])
 
     def each(count, fn):
         for d in range(1, count):
@@ -457,6 +455,16 @@
     def each_far(count, fn):
         for d in range(count - 1, 0, -1):
             fn(d)
+
+    def scaled(total, rank):
+        inv = invv[rrow(rank)]
+        return jnp.concatenate(
+            [
+                total[:, j * lanes : (j + 1) * lanes] * inv
+                for j in range(total.shape[1] // lanes)
+            ],
+            axis=1,
+        )
 
     zmasks = list(range(2, n, 2))
     nb = prop
@@ -472,33 +480,24 @@
         ssq[sl, :] = (accs4[0] + accs4[1]) + (accs4[2] + accs4[3])
         return c
 
-    for i in range(chunks):
-        in_tok[i].wait()
-        if i == chunks - 1:
-            for c in copies[-3:]:
-                c.start()
-        lax.fori_loop(i * crow // nb, (i + 1) * crow // nb, sum_rows, 0)
-    total = dot_hi(ssq[...], jnp.ones((lanes, lanes), F32))
-    inv = lax.rsqrt(total / width + epsilon)
-    invv[...] = inv
+    in_x.wait()
     in_gain.wait()
-    for j in range(kdim // lanes):
-        at = pl.ds(pl.multiple_of(me * kdim + j * lanes, lanes), lanes)
-        xloc[:, j * lanes : (j + 1) * lanes] = (
-            tokv[:, at].astype(F32) * inv * gain[:, at]
-        ).astype(BF)
+    xloc[...] = (xraw[...].astype(F32) * gain[:, mine]).astype(BF)
     in_wq.wait()
     part_q[...] = jnp.dot(xloc[...], wqkv[0], preferred_element_type=F32).astype(BF)
     pl.semaphore_wait(barrier, everyone - 1)
     for m in zmasks[::-1] + [0]:
         q_yrs(m).start()
+    for c in copies[urgent:]:
+        c.start()
     in_wk.wait()
     in_wv.wait()
     part_kv[:, 0:hw] = jnp.dot(xloc[...], wqkv[1], preferred_element_type=F32).astype(BF)
     part_kv[:, hw : 2 * hw] = jnp.dot(xloc[...], wqkv[2], preferred_element_type=F32).astype(BF)
+    def kv_sum(m):
+        return part_kv[rrow(kvs[m ^ last])].astype(F32) + kv_y[m // 2].astype(F32)
     for m in zmasks[::-1] + [0]:
         kv_yrs(m).start()
-
     in_lens.wait()
     in_accs.wait()
     in_cum.wait()
@@ -524,7 +523,14 @@
     take = hot(iota((num_seqs, r64), 1) // heads == iota((num_seqs, r64), 0))
     cflat = dot_hi(take, e1)
     brow[...] = jnp.where(iota((num_seqs, cols), 1) // heads < rel16, -cflat, floor_value)
-
+    for m in zmasks[::-1]:
+        q_yrs(m).wait_recv()
+        q_zs[m // 2] = (part_q[rrow(kvs[m])].astype(F32) + q_y[m // 2].astype(F32)).astype(BF)
+        q_zrs(m).start()
+    in_tok.wait()
+    lax.fori_loop(0, rows // nb, sum_rows, 0)
+    total = dot_hi(ssq[...], jnp.ones((lanes, lanes), F32))
+    invv[...] = lax.rsqrt(total / width + epsilon)
     in_parent.wait()
     ri = iota((rows, rows), 0)
     ci = iota((rows, rows), 1)
@@ -541,46 +547,14 @@
         low = a.astype(BF)
         a = jnp.minimum(jnp.dot(low, low, preferred_element_type=F32), 1.0)
     anc[...] = a
-    for m in zmasks[::-1]:
-        q_yrs(m).wait_recv()
-        q_zs[m // 2] = (part_q[rrow(kvs[m])].astype(F32) + q_y[m // 2].astype(F32)).astype(BF)
-        q_zrs(m).start()
-    in_wft.wait()
-    in_bias.wait()
-    wscaled = wft[...].astype(F32) * gain[...]
-    whigh = wscaled.astype(BF)
-    wlow = (wscaled - whigh.astype(F32)).astype(BF)
-    lf = lax.dot_general(
-        jnp.concatenate([whigh, wlow], axis=0), tokv[...], NT, preferred_element_type=F32
-    )
-    lf = lf[0:heads_all] + lf[heads_all : 2 * heads_all]
-    inv_lane = dot_hi(jnp.full((8, lanes), 1.0 / lanes, F32), invv[...], NT)[0:1]
-    bcol = jnp.zeros((heads_all, rows), F32)
-    for h in range(heads_all):
-        bcol = jnp.where(iota((heads_all, rows), 0) == h, bias[h], bcol)
-    z = lf * inv_lane + bcol
-    lf = jnp.minimum(z, 0.0) - jnp.log1p(jnp.exp(-jnp.abs(z)))
-    path_t = dot_hi(lf, a, NT)
-    rep = hot(iota((r64, heads_all), 1) == mt * heads + iota((r64, heads_all), 0) % heads)
-    pm = dot_hi(rep, path_t)
-    pm = jnp.where(iota((r64, rows), 1) // prop == iota((r64, rows), 0) // heads, pm, 0.0)
-    fold = hot(iota((rows, 128), 0) % prop == iota((rows, 128), 1) % prop)
-    pt = dot_hi(pm, fold)
-    ptile[...] = pt
-    ptm = jnp.where((iota((r64, 128), 1) // prop) % heads == iota((r64, 128), 0) % heads, pt, 0.0)
-    tpath[...] = dot_hi(take, ptm)
-    in_kc.wait()
-    in_vc.wait()
-
     q_yrs(0).wait_recv()
     own = part_q[rrow(me)].astype(F32) + q_y[0].astype(F32)
     received(on_qz, q_zr.at[pl.ds(1, half - 1)])
     for m in zmasks:
         own = own + q_zr[m // 2].astype(F32)
-    q_full[rrow(me)] = own.astype(BF)
+    q_full[rrow(me)] = scaled(own, me).astype(BF)
     for m in [1] + zmasks[::-1]:
         q_ag(m).start()
-
     same_head = iota((hp, cols), 0) // prop == iota((hp, cols), 1) % heads
     diag_l = iota((L, L), 0) == iota((L, L), 1)
 
@@ -622,38 +596,62 @@
             if m != last:
                 stat_copy(last - m).start()
                 val_copy(last - m).start()
-
-    blocks([0])
-    for m in zmasks[::-1]:
-        kv_yrs(m).wait_recv()
-        kv_zs[m // 2] = (
-            part_kv[rrow(kvs[m ^ last])].astype(F32) + kv_y[m // 2].astype(F32)
-        ).astype(BF)
-        kv_zrs(m).start()
-
     def take_q(m):
         q_ag(m).wait_recv()
         if m % 2 == 0:
             q_ag(m + 1).start()
-
+    in_kc.wait()
+    in_vc.wait()
+    blocks([0])
+    for i, m in enumerate((2, 6)):
+        kv_yrs(m).wait_recv()
+        kv_zs[i] = kv_sum(m).astype(BF)
+    kv_near().start()
+    in_wft.wait()
+    in_bias.wait()
+    wscaled = wft[...].astype(F32) * gain[...]
+    whigh = wscaled.astype(BF)
+    wlow = (wscaled - whigh.astype(F32)).astype(BF)
+    lf = lax.dot_general(
+        jnp.concatenate([whigh, wlow], axis=0), tokv[...], NT, preferred_element_type=F32
+    )
+    lf = lf[0:heads_all] + lf[heads_all : 2 * heads_all]
+    inv_lane = dot_hi(jnp.full((8, lanes), 1.0 / lanes, F32), invv[...], NT)[0:1]
+    bcol = jnp.zeros((heads_all, rows), F32)
+    for h in range(heads_all):
+        bcol = jnp.where(iota((heads_all, rows), 0) == h, bias[h], bcol)
+    z = lf * inv_lane + bcol
+    lf = jnp.minimum(z, 0.0) - jnp.log1p(jnp.exp(-jnp.abs(z)))
+    path_t = dot_hi(lf, a, NT)
+    rep = hot(iota((r64, heads_all), 1) == mt * heads + iota((r64, heads_all), 0) % heads)
+    pm = dot_hi(rep, path_t)
+    pm = jnp.where(iota((r64, rows), 1) // prop == iota((r64, rows), 0) // heads, pm, 0.0)
+    fold = hot(iota((rows, 128), 0) % prop == iota((rows, 128), 1) % prop)
+    pt = dot_hi(pm, fold)
+    ptile[...] = pt
+    ptm = jnp.where((iota((r64, 128), 1) // prop) % heads == iota((r64, 128), 0) % heads, pt, 0.0)
+    tpath[...] = dot_hi(take, ptm)
     take_q(2)
     take_q(1)
     blocks([1, 2])
     take_q(4)
     take_q(6)
     blocks([4, 6])
+    kv_yrs(4).wait_recv()
+    kv_near().wait_recv()
+    kv_zs[2] = (kv_sum(4) + kv_zr[1].astype(F32)).astype(BF)
+    kv_far().start()
     take_q(3)
     take_q(5)
     blocks([3, 5])
     take_q(7)
     blocks([7])
 
+
     kv_yrs(0).wait_recv()
-    own = part_kv[rrow(kvs[last])].astype(F32) + kv_y[0].astype(F32)
-    received(on_kz, kv_zr.at[pl.ds(1, half - 1)])
-    for m in zmasks:
-        own = own + kv_zr[m // 2].astype(F32)
-    kv_full[rrow(kvs[last])] = own.astype(BF)
+    kv_far().wait_recv()
+    own = kv_sum(0) + kv_zr[0].astype(F32) + kv_zr[2].astype(F32)
+    kv_full[rrow(kvs[last])] = scaled(own, kvs[last]).astype(BF)
 
     fold_h = iota((rows, hp), 0)
     tmax, ttot, tval = [], [], []
@@ -747,7 +745,7 @@
 
     def o_copy(g, d):
         return send(
-            10,
+            11,
             on_o + g,
             {"tp": tps[d]},
             o_send.at[tps[d], grows[g]],
@@ -783,7 +781,7 @@
 
     def sq_copy(e):
         peer = {"kv": kvs[e // nt], "tp": tps[e % nt]}
-        return send(11, on_sq, peer, sq_send, sq_recv.at[e])
+        return send(12, on_sq, peer, sq_send, sq_recv.at[e])
 
     each_far(everyone, lambda e: sq_copy(e).start())
 
@@ -827,91 +825,91 @@
     sent(0, q_y)
     sent(1, q_zr.at[pl.ds(1, half - 1)])
     sent(2, kv_y)
-    sent(3, kv_zr.at[pl.ds(1, half - 1)])
-    sent(4, q_full.at[pl.ds(0, last * R)])
-    sent(5, cand_recv.at[pl.ds(1, last)])
-    sent(6, st_recv.at[pl.ds(1, last)])
-    sent(7, val_recv.at[pl.ds(1, last)])
-    sent(8, att.at[pl.ds(0, last * R)])
+    sent(3, kv_zr.at[pl.ds(0, 2)])
+    sent(4, kv_zr.at[2])
+    sent(5, q_full.at[pl.ds(0, last * R)])
+    sent(6, cand_recv.at[pl.ds(1, last)])
+    sent(7, st_recv.at[pl.ds(1, last)])
+    sent(8, val_recv.at[pl.ds(1, last)])
+    sent(9, att.at[pl.ds(0, last * R)])
 
     @pl.when(upper)
     def _():
-        sent(9, kv_full.at[pl.ds(0, (2 + half) * R)])
+        sent(10, kv_full.at[pl.ds(0, (2 + half) * R)])
 
     @pl.when(jnp.logical_not(upper))
     def _():
-        sent(9, kv_full.at[pl.ds(0, R)])
-
-    sent(10, o_recv.at[pl.ds(1, nt - 1)])
-    sent(11, sq_recv.at[pl.ds(1, everyone - 1)])
+        sent(10, kv_full.at[pl.ds(0, R)])
+
+    sent(11, o_recv.at[pl.ds(1, nt - 1)])
+    sent(12, sq_recv.at[pl.ds(1, everyone - 1)])
 
 
 def patch_kernel(
-    n, prop, kc, vc, knew, vnew, mixed, cum, lens, accs, k_out, v_out, mixed_out, cum_out, sem, bsem, wsem
+    n,
+    prop,
+    k_in,
+    v_in,
+    knew,
+    vnew,
+    mixed,
+    cum,
+    lens,
+    accs,
+    k_out,
+    v_out,
+    mixed_out,
+    cum_out,
+    k_buf,
+    v_buf,
+    sem,
 ):
     me = lax.axis_index("kv")
     num_seqs, span = k_out.shape[:2]
     out_m = pltpu.make_async_copy(mixed, mixed_out, sem.at[0])
     out_c = pltpu.make_async_copy(cum, cum_out, sem.at[1])
-    bulk = [
-        [
-            pltpu.make_async_copy(src.at[s], dst.at[s], bsem.at[i, s])
-            for i, (src, dst) in enumerate(((kc, k_out), (vc, v_out)))
-        ]
-        for s in range(num_seqs)
-    ]
-    for row in bulk:
-        for c in row:
-            c.start()
     out_m.start()
     out_c.start()
 
-    def moves(act, before=None):
-        for s in range(num_seqs):
-            if before is not None:
-                before(s)
-            at = lens[s] + accs[s] - me * span
-            pairs = ((knew, k_out), (vnew, v_out))
-
-            @pl.when((at >= 0) & (at <= span - prop))
-            def _():
-                for i, (src, dst) in enumerate(pairs):
-                    act(
-                        pltpu.make_async_copy(
-                            src.at[s], dst.at[s, pl.ds(at, prop)], wsem.at[i, s]
-                        )
-                    )
-
-            @pl.when(((at > -prop) & (at < 0)) | ((at > span - prop) & (at < span)))
-            def _():
-                def one(j, c):
-                    @pl.when((at + j >= 0) & (at + j < span))
-                    def _():
-                        for i, (src, dst) in enumerate(pairs):
-                            act(
-                                pltpu.make_async_copy(
-                                    src.at[s, j], dst.at[s, at + j], wsem.at[i, s]
-                                )
-                            )
-
-                    return c
-
-                lax.fori_loop(0, prop, one, 0)
-
-    def settle(s):
-        for c in bulk[s]:
-            c.wait()
+    def store(s):
+        pltpu.make_async_copy(k_buf.at[s], k_out.at[s], sem.at[2]).start()
+        pltpu.make_async_copy(v_buf.at[s], v_out.at[s], sem.at[3]).start()
+
+    def place(s):
+        at = lens[s] + accs[s] - me * span
+
+        @pl.when((at >= 0) & (at <= span - prop))
+        def _():
+            k_buf[s, pl.ds(at, prop)] = knew[s]
+            v_buf[s, pl.ds(at, prop)] = vnew[s]
+
+        @pl.when(((at > -prop) & (at < 0)) | ((at > span - prop) & (at < span)))
+        def _():
+            def one(j, c):
+                @pl.when((at + j >= 0) & (at + j < span))
+                def _():
+                    k_buf[s, pl.ds(at + j, 1)] = knew[s, pl.ds(j, 1)]
+                    v_buf[s, pl.ds(at + j, 1)] = vnew[s, pl.ds(j, 1)]
+
+                return c
+
+            lax.fori_loop(0, prop, one, 0)
 
     @pl.when(me >= n // 2)
     def _():
-        moves(lambda c: c.start(), settle)
-        moves(lambda c: c.wait())
+        for s in range(num_seqs):
+            place(s)
+            if s > 0:
+                store(s - 1)
+        store(num_seqs - 1)
 
     @pl.when(me < n // 2)
     def _():
         for s in range(num_seqs):
-            settle(s)
-
+            store(s)
+
+    pltpu.make_async_copy(k_buf, k_out, sem.at[2]).wait()
+    pltpu.make_async_copy(v_buf, v_out, sem.at[3]).wait()
     out_m.wait()
     out_c.wait()
 
@@ -982,6 +980,7 @@
             V((rows, 128), F32),
             V((rows, 128), F32),
             V((rows, w_query.shape[0]), BF),
+            V((rows, w_query.shape[0]), BF),
             V((rows, hw), BF),
             V((half, R, hw), BF),
             V((half, R, hw), BF),
@@ -989,8 +988,8 @@
             V((rows, hw), BF),
             V((rows, 2 * hw), BF),
             V((half, R, 2 * hw), BF),
-            V((half, R, 2 * hw), BF),
-            V((half, R, 2 * hw), BF),
+            V((half - 1, R, 2 * hw), BF),
+            V((half - 1, R, 2 * hw), BF),
             V((rows, 2 * hw), BF),
             V((n, 2, L), F32),
             V((n, L, hd), BF),
@@ -1007,9 +1006,9 @@
             V((nt, rows, oc), BF),
             V((1, rows), F32),
             V((everyone, 1, rows), F32),
-            D((18,)),
-            D((12,)),
-            D((2 * half + 4 * n + 7,)),
+            D((16,)),
+            D((13,)),
+            D((2 * half + 4 * n + 8,)),
         ],
         compiler_params=pltpu.CompilerParams(
             collective_id=0, has_side_effects=True, vmem_limit_bytes=50 * 1024 * 1024
@@ -1038,17 +1037,20 @@
         ]
     )
     fresh = (num_seqs, prop, heads, hd)
-    key_out, value_out, mixed, cum_new = pl.pallas_call(
+    key_out, value_out, mixed, cum_new, *unused = pl.pallas_call(
         functools.partial(patch_kernel, n, prop),
         out_shape=(
             pltpu.HBM(key_cache.shape, BF),
             pltpu.HBM(value_cache.shape, BF),
             pltpu.HBM(mixed.shape, BF),
             pltpu.HBM(cum.shape, F32),
+            V(key_cache.shape, BF),
+            V(key_cache.shape, BF),
         ),
         in_specs=[vmem, vmem, vmem, vmem, vmem, vmem, smem, smem],
-        out_specs=(hbm, hbm, hbm, hbm),
-        scratch_shapes=[D((2,)), D((2, num_seqs)), D((2, num_seqs))],
+        out_specs=(hbm, hbm, hbm, hbm, vmem, vmem),
+        input_output_aliases={0: 4, 1: 5},
+        scratch_shapes=[D((4,))],
         compiler_params=pltpu.CompilerParams(
             has_side_effects=True, vmem_limit_bytes=4 * 1024 * 1024
         ),

time: 51.7 us -> 49.5 us (0.957)
  Pallas kernels: 50.8 us -> 48.7 us
    pallas_call x1, Pallas kernels: 47.7 us -> 46.1 us  [fast_device(): pl.pallas_call(functools.partial(layer_kernel, n, nt, num_seqs, prop, hea...]
    pallas_call x1, Pallas kernels: 3.14 us -> 2.59 us  [fast_device(): pl.pallas_call(functools.partial(patch_kernel, n, prop), out_shape=(pltpu...]
where the time goes in v5:
time: 49.5 us; the launch traced here: 49.4 us
  Pallas kernels  48.7 us (98%)
  between operations  0.68 us (1%)
    pallas_call x1, Pallas kernels, fast_device(): pl.pallas_call(functools.partial(layer_kernel, n, nt, num_seqs, prop, hea...  46.1 us
    pallas_call x1, Pallas kernels, fast_device(): pl.pallas_call(functools.partial(patch_kernel, n, prop), out_shape=(pltpu...  2.59 us

profile of v5, /device:TPU:0, one launch (start us, length us, event | category | flops | bytes accessed | tf_op | source)
XLA Modules:
  0.0 49.4 jit_solution(4254905581908677359)
XLA Ops:
  0.6 0.0 copy-start
  0.6 0.0 copy-start.1
  0.7 46.1 %layer.1 = (bf16[256,128]{1,0:T(8,128)(2,1)S(1)}, f32[64,128]{1,0:T(8,128)S(1)}, bf16[16,64,128]{2,1,0:T(8,128)(2,1)S(1)}, bf16[16,64,128]{2,1,0:T(8,128)(2,1)S(...) custom-call(bf16[256,4096]{1,0:T(8,128)(2,1)} %bitcast.21, f32[1,4096]{1,0:T(1,128)} %bitcast.26, ...), custom_call_target="tpu_custom_call" | custom-call | tf_op jit(solution)/shard_map/layer/pallas_call | solution.py:956
  46.8 0.0 copy-done
  46.8 0.0 copy-done.1
  46.8 2.6 %patch.1 = (bf16[16,128,4,128]{3,2,1,0:T(4,128)(2,1)}, bf16[16,128,4,128]{3,2,1,0:T(4,128)(2,1)}, bf16[256,128]{1,0:T(8,128)(2,1)}, f32[64,128]{1,0:T(8,128)}, b...) custom-call(bf16[16,128,4,128]{3,2,1,0:T(4,128)(2,1)S(1)} %bitcast.1, ...), custom_call_target="tpu_custom_call", output_to_operand_aliasing={{4}: (0, {}), {5}: (1, {})} | custom-call | tf_op jit(solution)/shard_map/patch/pallas_call | solution.py:1040
Async XLA Ops:
  0.6 46.1 %copy-start = (s32[16]{0:T(128)S(1)}, s32[16]{0:T(128)}, u32[]{:S(2)}) copy-start(s32[16]{0:T(128)} %lens.1) | copy-start | bytes 196
  0.6 46.1 %copy-start.1 = (s32[16]{0:T(128)S(1)}, s32[16]{0:T(128)}, u32[]{:S(2)}) copy-start(s32[16]{0:T(128)} %accs.1) | copy-start | bytes 196

commit v6 on v5

--- a/solution.py
+++ b/solution.py
@@ -254,6 +254,7 @@
     vnew_out,
     kcv,
     vcv,
+    at_out,
     tokv,
     gain,
     wqkv,
@@ -510,6 +511,7 @@
     s16 = iota((num_seqs, cols), 0)
     for s in range(num_seqs):
         rel_s = lens[s] + accs[s] - base
+        at_out[s] = rel_s
         rel64 = jnp.where(srow == s, rel_s, rel64)
         rel16 = jnp.where(s16 == s, rel_s, rel16)
     cand = jnp.max(jnp.where(lane == rel64 - 1, c64, floor_value), axis=1, keepdims=True)
@@ -854,8 +856,7 @@
     vnew,
     mixed,
     cum,
-    lens,
-    accs,
+    starts,
     k_out,
     v_out,
     mixed_out,
@@ -876,7 +877,7 @@
         pltpu.make_async_copy(v_buf.at[s], v_out.at[s], sem.at[3]).start()
 
     def place(s):
-        at = lens[s] + accs[s] - me * span
+        at = starts[s]
 
         @pl.when((at >= 0) & (at <= span - prop))
         def _():
@@ -953,7 +954,7 @@
     V = pltpu.VMEM
     S = pltpu.SMEM
     D = pltpu.SemaphoreType.DMA
-    mixed, cum_new, knew, vnew, kv, vv = pl.pallas_call(
+    mixed, cum_new, knew, vnew, kv, vv, starts = pl.pallas_call(
         functools.partial(layer_kernel, n, nt, num_seqs, prop, heads, hd, span),
         out_shape=(
             V((rows, oc), BF),
@@ -962,9 +963,10 @@
             V((num_seqs, heads * prop, hd), BF),
             V(kc.shape, BF),
             V(vc.shape, BF),
+            S(lengths.shape, jnp.int32),
         ),
         in_specs=[hbm] * 15,
-        out_specs=(vmem,) * 6,
+        out_specs=(vmem,) * 6 + (smem,),
         scratch_shapes=[
             V((rows, width), BF),
             V((1, width), F32),
@@ -1047,7 +1049,7 @@
             V(key_cache.shape, BF),
             V(key_cache.shape, BF),
         ),
-        in_specs=[vmem, vmem, vmem, vmem, vmem, vmem, smem, smem],
+        in_specs=[vmem, vmem, vmem, vmem, vmem, vmem, smem],
         out_specs=(hbm, hbm, hbm, hbm, vmem, vmem),
         input_output_aliases={0: 4, 1: 5},
         scratch_shapes=[D((4,))],
@@ -1060,8 +1062,7 @@
             pltpu.with_memory_space_constraint(operand, V)
             for operand in (kv.reshape(key_cache.shape), vv.reshape(key_cache.shape), knew.reshape(fresh), vnew.reshape(fresh), mixed, cum_new)
         ],
-        lengths,
-        accepted,
+        starts,
     )
     cum_out = jnp.swapaxes(cum_new.reshape(num_seqs, heads, span), 1, 2)
     return (

time: 49.5 us -> 48.9 us (0.988)
  Pallas kernels: 48.7 us -> 48.2 us
    pallas_call x1, Pallas kernels: 2.59 us -> 2.05 us  [fast_device(): pl.pallas_call(functools.partial(patch_kernel, n, prop), out_shape=(pltpu...]
where the time goes in v6:
time: 48.9 us; the launch traced here: 48.8 us
  Pallas kernels  48.2 us (99%)
  between operations  0.65 us (1%)
    pallas_call x1, Pallas kernels, fast_device(): pl.pallas_call(functools.partial(layer_kernel, n, nt, num_seqs, prop, hea...  46.1 us
    pallas_call x1, Pallas kernels, fast_device(): pl.pallas_call(functools.partial(patch_kernel, n, prop), out_shape=(pltpu...  2.05 us

profile of v6, /device:TPU:0, one launch (start us, length us, event | category | flops | bytes accessed | tf_op | source)
XLA Modules:
  0.0 48.8 jit_solution(7733378498539681348)
XLA Ops:
  0.6 46.1 %layer.1 = (bf16[256,128]{1,0:T(8,128)(2,1)S(1)}, f32[64,128]{1,0:T(8,128)S(1)}, bf16[16,64,128]{2,1,0:T(8,128)(2,1)S(1)}, bf16[16,64,128]{2,1,0:T(8,128)(2,1)S(...) custom-call(bf16[256,4096]{1,0:T(8,128)(2,1)} %bitcast.21, ...), custom_call_target="tpu_custom_call" | custom-call | tf_op jit(solution)/shard_map/layer/pallas_call | solution.py:957
  46.7 2.1 %patch.1 = (bf16[16,128,4,128]{3,2,1,0:T(4,128)(2,1)}, bf16[16,128,4,128]{3,2,1,0:T(4,128)(2,1)}, bf16[256,128]{1,0:T(8,128)(2,1)}, f32[64,128]{1,0:T(8,128)}, b...) custom-call(bf16[16,128,4,128]{3,2,1,0:T(4,128)(2,1)S(1)} %bitcast.1, ...), custom_call_target="tpu_custom_call", output_to_operand_aliasing={{4}: (0, {}), {5}: (1, {})} | custom-call | tf_op jit(solution)/shard_map/patch/pallas_call | solution.py:1042

commit v7 on v6

--- a/solution.py
+++ b/solution.py
@@ -213,6 +213,14 @@
 
 
 NT = (((1,), (1,)), ((), ()))
+TN = (((0,), (0,)), ((), ()))
+
+
+def thirds(x):
+    high = x.astype(BF)
+    rest = x - high.astype(F32)
+    middle = rest.astype(BF)
+    return high, middle, (rest - middle.astype(F32)).astype(BF)
 
 
 def flips(value, count):
@@ -401,8 +409,8 @@
         return flat[0] - count
 
     on_qy, on_qz, on_ky, on_kz = slots(half), slots(1), slots(half), slots(2)
-    on_qag, on_cand, on_stat, on_val = slots(n), slots(1), slots(1), slots(n)
-    on_att, on_kvag, on_o, on_sq = slots(n), slots(n), slots(2), slots(1)
+    on_qag, on_cand, on_stat, on_val = slots(n - 1), slots(1), slots(1), slots(n - 1)
+    on_att, on_kvag, on_o, on_sq = slots(half + 1), slots(half), slots(2), slots(1)
     last = n - 1
 
     def q_yrs(m):
@@ -423,8 +431,8 @@
 
     def q_ag(m):
         if m % 2:
-            return spread_to(5, on_qag + m, 1, q_full, kvs[m - 1])
-        return spread_to(5, on_qag + m, m, q_full, me)
+            return spread_to(5, on_qag + m - 1, 1, q_full, kvs[m - 1])
+        return spread_to(5, on_qag + m - 1, m, q_full, me)
 
     def cand_copy(m):
         return to_kv(6, on_cand, m, cand_send, cand_recv.at[m])
@@ -433,21 +441,21 @@
         return to_kv(7, on_stat, m, st_send.at[m], st_recv.at[m])
 
     def val_copy(m):
-        return to_kv(8, on_val + m, m, val_send.at[m], val_recv.at[m])
+        return to_kv(8, on_val + m - 1, m, val_send.at[m], val_recv.at[m])
 
     def att_ag(m):
         if m % 2:
-            return spread_to(9, on_att + m, 1, att, kvs[(m - 1) ^ last])
-        return spread_to(9, on_att + m, m, att, kvs[last])
+            return spread_to(9, on_att + half - 1 + m // half, 1, att, kvs[(m - 1) ^ last])
+        return spread_to(9, on_att + m // 2 - 1, m, att, kvs[last])
 
     def kv_cross():
-        return spread_to(10, on_kvag + half, half, kv_full, kvs[last])
+        return spread_to(10, on_kvag, half, kv_full, kvs[last])
 
     def kv_pass(m):
-        return spread_to(10, on_kvag + m, half // 2, kv_full, kvs[(m - half // 2) ^ last])
+        return spread_to(10, on_kvag + 1 + m // half, half // 2, kv_full, kvs[(m - half // 2) ^ last])
 
     def kv_side(m):
-        return spread_to(10, on_kvag + m, 1, kv_full, kvs[(m - 1) ^ last])
+        return spread_to(10, on_kvag + half - 1, 1, kv_full, kvs[(m - 1) ^ last])
 
     def each(count, fn):
         for d in range(1, count):
@@ -758,8 +766,7 @@
         att_ag(m).wait_recv()
         att_ag(m + 1).start()
     for g in range(2):
-        for m in range(1 + g * half, (g + 1) * half, 2):
-            att_ag(m).wait_recv()
+        received(on_att + half - 1 + g, att.at[pl.ds(0, half // 2 * R)])
         full = jnp.dot(att[grows[g]], wov[...], preferred_element_type=F32).astype(BF)
         for t in range(nt):
             o_send[t, grows[g]] = full[:, t * oc : (t + 1) * oc]
@@ -778,7 +785,11 @@
         received(on_o + g, o_recv.at[pl.ds(1, nt - 1), grows[g]])
     for d in range(1, nt):
         mixed = mixed + o_recv[d].astype(F32)
-    sq = dot_hi(jnp.ones((8, oc), F32), mixed * mixed, NT)[0:1]
+    ones = jnp.ones((8, oc), BF)
+    sq = sum(
+        lax.dot_general(ones, part, NT, preferred_element_type=F32)
+        for part in thirds(mixed * mixed)
+    )[0:1]
     sq_send[...] = sq
 
     def sq_copy(e):
@@ -797,8 +808,7 @@
     def _():
         kv_pass(6).wait_recv()
         kv_side(7).start()
-        for m in range(1, n, 2):
-            kv_side(m).wait_recv()
+        received(on_kvag + half - 1, kv_full.at[pl.ds(0, half * R)])
 
         def some(i, c):
             fresh = [
@@ -818,8 +828,10 @@
     received(on_sq, sq_recv.at[pl.ds(1, everyone - 1)])
     for e in range(1, everyone):
         sq = sq + sq_recv[e]
-    ssum = dot_hi(
-        jnp.broadcast_to(sq, (8, rows)), jnp.full((8, oc), 0.125, F32), (((0,), (0,)), ((), ()))
+    eighth = jnp.full((8, oc), 0.125, BF)
+    ssum = sum(
+        lax.dot_general(part, eighth, TN, preferred_element_type=F32)
+        for part in thirds(jnp.broadcast_to(sq, (8, rows)))
     )
     in_gpost.wait()
     mixed_out[...] = (mixed * lax.rsqrt(ssum / width + epsilon) * gpost[...]).astype(BF)
@@ -1010,7 +1022,7 @@
             V((everyone, 1, rows), F32),
             D((16,)),
             D((13,)),
-            D((2 * half + 4 * n + 8,)),
+            D((4 * half + 2 * n + 7,)),
         ],
         compiler_params=pltpu.CompilerParams(
             collective_id=0, has_side_effects=True, vmem_limit_bytes=50 * 1024 * 1024

time: 48.9 us -> 48.6 us (level)
  no operation moved by 1% of the time
where the time goes in v7:
time: 48.6 us; the launch traced here: 48.5 us
  Pallas kernels  47.9 us (99%)
  between operations  0.65 us (1%)
    pallas_call x1, Pallas kernels, fast_device(): pl.pallas_call(functools.partial(layer_kernel, n, nt, num_seqs, prop, hea...  45.8 us
    pallas_call x1, Pallas kernels, fast_device(): pl.pallas_call(functools.partial(patch_kernel, n, prop), out_shape=(pltpu...  2.05 us

profile of v7, /device:TPU:0, one launch (start us, length us, event | category | flops | bytes accessed | tf_op | source)
XLA Modules:
  0.0 48.5 jit_solution(10340670059205698382)
XLA Ops:
  0.6 45.8 %layer.1 = (bf16[256,128]{1,0:T(8,128)(2,1)S(1)}, f32[64,128]{1,0:T(8,128)S(1)}, bf16[16,64,128]{2,1,0:T(8,128)(2,1)S(1)}, bf16[16,64,128]{2,1,0:T(8,128)(2,1)S(...) custom-call(bf16[256,4096]{1,0:T(8,128)(2,1)} %bitcast.21, ...), custom_call_target="tpu_custom_call" | custom-call | tf_op jit(solution)/shard_map/layer/pallas_call | solution.py:969
  46.4 2.1 %patch.1 = (bf16[16,128,4,128]{3,2,1,0:T(4,128)(2,1)}, bf16[16,128,4,128]{3,2,1,0:T(4,128)(2,1)}, bf16[256,128]{1,0:T(8,128)(2,1)}, f32[64,128]{1,0:T(8,128)}, b...) custom-call(bf16[16,128,4,128]{3,2,1,0:T(4,128)(2,1)S(1)} %bitcast.1, ...), custom_call_target="tpu_custom_call", output_to_operand_aliasing={{4}: (0, {}), {5}: (1, {})} | custom-call | tf_op jit(solution)/shard_map/patch/pallas_call | solution.py:1054

commit v8 on v7

--- a/solution.py
+++ b/solution.py
@@ -221,6 +221,19 @@
     rest = x - high.astype(F32)
     middle = rest.astype(BF)
     return high, middle, (rest - middle.astype(F32)).astype(BF)
+
+
+NN = (((1,), (0,)), ((), ()))
+
+
+def dot_left(x, exact, dims=NN):
+    exact = exact.astype(BF)
+    return sum(lax.dot_general(p, exact, dims, preferred_element_type=F32) for p in thirds(x))
+
+
+def dot_right(exact, y, dims=NN):
+    exact = exact.astype(BF)
+    return sum(lax.dot_general(exact, p, dims, preferred_element_type=F32) for p in thirds(y))
 
 
 def flips(value, count):
@@ -539,7 +552,7 @@
         q_zrs(m).start()
     in_tok.wait()
     lax.fori_loop(0, rows // nb, sum_rows, 0)
-    total = dot_hi(ssq[...], jnp.ones((lanes, lanes), F32))
+    total = dot_left(ssq[...], jnp.ones((lanes, lanes), F32))
     invv[...] = lax.rsqrt(total / width + epsilon)
     in_parent.wait()
     ri = iota((rows, rows), 0)
@@ -626,21 +639,21 @@
         jnp.concatenate([whigh, wlow], axis=0), tokv[...], NT, preferred_element_type=F32
     )
     lf = lf[0:heads_all] + lf[heads_all : 2 * heads_all]
-    inv_lane = dot_hi(jnp.full((8, lanes), 1.0 / lanes, F32), invv[...], NT)[0:1]
+    inv_lane = dot_right(jnp.full((8, lanes), 1.0 / lanes, F32), invv[...], NT)[0:1]
     bcol = jnp.zeros((heads_all, rows), F32)
     for h in range(heads_all):
         bcol = jnp.where(iota((heads_all, rows), 0) == h, bias[h], bcol)
     z = lf * inv_lane + bcol
     lf = jnp.minimum(z, 0.0) - jnp.log1p(jnp.exp(-jnp.abs(z)))
-    path_t = dot_hi(lf, a, NT)
+    path_t = dot_left(lf, a, NT)
     rep = hot(iota((r64, heads_all), 1) == mt * heads + iota((r64, heads_all), 0) % heads)
-    pm = dot_hi(rep, path_t)
+    pm = dot_right(rep, path_t)
     pm = jnp.where(iota((r64, rows), 1) // prop == iota((r64, rows), 0) // heads, pm, 0.0)
     fold = hot(iota((rows, 128), 0) % prop == iota((rows, 128), 1) % prop)
-    pt = dot_hi(pm, fold)
+    pt = dot_left(pm, fold)
     ptile[...] = pt
     ptm = jnp.where((iota((r64, 128), 1) // prop) % heads == iota((r64, 128), 0) % heads, pt, 0.0)
-    tpath[...] = dot_hi(take, ptm)
+    tpath[...] = dot_right(take, ptm)
     take_q(2)
     take_q(1)
     blocks([1, 2])

time: 48.6 us -> 49.6 us (1.021)
  Pallas kernels: 47.9 us -> 48.8 us
    pallas_call x1, Pallas kernels: 45.8 us -> 46.8 us  [fast_device(): pl.pallas_call(functools.partial(layer_kernel, n, nt, num_seqs, prop, hea...]
where the time goes in v8:
time: 49.6 us; the launch traced here: 49.5 us
  Pallas kernels  48.8 us (98%)
  between operations  0.65 us (1%)
    pallas_call x1, Pallas kernels, fast_device(): pl.pallas_call(functools.partial(layer_kernel, n, nt, num_seqs, prop, hea...  46.8 us
    pallas_call x1, Pallas kernels, fast_device(): pl.pallas_call(functools.partial(patch_kernel, n, prop), out_shape=(pltpu...  2.05 us

profile of v8, /device:TPU:0, one launch (start us, length us, event | category | flops | bytes accessed | tf_op | source)
XLA Modules:
  0.0 49.5 jit_solution(13499666716639065111)
XLA Ops:
  0.6 46.8 %layer.1 = (bf16[256,128]{1,0:T(8,128)(2,1)S(1)}, f32[64,128]{1,0:T(8,128)S(1)}, bf16[16,64,128]{2,1,0:T(8,128)(2,1)S(1)}, bf16[16,64,128]{2,1,0:T(8,128)(2,1)S(...) custom-call(bf16[256,4096]{1,0:T(8,128)(2,1)} %bitcast.21, ...), custom_call_target="tpu_custom_call" | custom-call | tf_op jit(solution)/shard_map/layer/pallas_call | solution.py:982
  47.4 2.1 %patch.1 = (bf16[16,128,4,128]{3,2,1,0:T(4,128)(2,1)}, bf16[16,128,4,128]{3,2,1,0:T(4,128)(2,1)}, bf16[256,128]{1,0:T(8,128)(2,1)}, f32[64,128]{1,0:T(8,128)}, b...) custom-call(bf16[16,128,4,128]{3,2,1,0:T(4,128)(2,1)S(1)} %bitcast.1, ...), custom_call_target="tpu_custom_call", output_to_operand_aliasing={{4}: (0, {}), {5}: (1, {})} | custom-call | tf_op jit(solution)/shard_map/patch/pallas_call | solution.py:1067
